TPU v7x, 32 devices: a whole 2x2x4 slice. The times are simulated.
32 devices in a mesh: sp: 16 (over z, y, x), tp: 2 (over core).
Axes of the slice: x: 2, y: 2, z: 4, core: 2. Of those that a mesh axis runs over, the one named last changes fastest.
Arguments:
- tokens: bfloat16 [4096, 2048], P('sp', 'tp'), may hold values from -6 to 6
- norm_gain: float32 [2048], replicated, may hold values from 0.1 to 1.9
- query_weight: bfloat16 [2048, 1024], P(None, 'tp'), may hold values from -0.18782524 to 0.18782524
- key_weight: bfloat16 [2048, 1024], P(None, 'tp'), may hold values from -0.18782524 to 0.18782524
- value_weight: bfloat16 [2048, 1024], P(None, 'tp'), may hold values from -0.125 to 0.125
- gate_weight: bfloat16 [2048, 1024], P(None, 'tp'), may hold values from -0.125 to 0.125
- outer_weight: bfloat16 [2048, 1024], P(None, 'tp'), may hold values from -0.125 to 0.125
- inner_weight: bfloat16 [2048, 1024], P(None, 'tp'), may hold values from -0.125 to 0.125
- signal_weight: bfloat16 [2048, 1024], P(None, 'tp'), may hold values from -0.125 to 0.125
- conv_taps: float32 [3, 1024], P(None, 'tp'), may hold values from -3.5 to 3.5
- lambdas: float32 [8], P('tp'), may hold values from 0.3 to 0.8
- head_gain: float32 [1024], P('tp'), may hold values from 0.1 to 1.9
- attn_out_weight: bfloat16 [1024, 2048], P('tp'), may hold values from -0.125 to 0.125
- conv_out_weight: bfloat16 [1024, 2048], P('tp'), may hold values from -0.125 to 0.125
Outputs:
- mixed: bfloat16 [4096, 2048], P(('sp', 'tp'))
- log_totals: float32 [8, 2, 4096], P('tp', None, 'sp')
All inputs are finite; a program needn't handle non-finite values.
Results may differ from a plain program's by a relative error of at most 0.014.
Values may be sent and summed in bfloat16 or wider, within the bound.
A program may use at most 128 MiB of HBM per device.

v0:
```python
import functools
import math

import jax
import jax.numpy as jnp
from jax import lax
from jax.experimental import pallas as pl
from jax.experimental.pallas import tpu as pltpu
from jax.sharding import PartitionSpec as P

MESH = pl.DeviceIdType.MESH


def passed_along(shard, axis, by):
    count = lax.axis_size(axis)
    pairs = [(i, i + by) for i in range(count) if 0 <= i + by < count]
    return lax.ppermute(shard, axis, pairs)


def per_device(
    tokens,
    norm_gain,
    query_weight,
    key_weight,
    value_weight,
    gate_weight,
    outer_weight,
    inner_weight,
    signal_weight,
    conv_taps,
    lambdas,
    head_gain,
    attn_out_weight,
    conv_out_weight,
):
    row_count = tokens.shape[0]
    width = norm_gain.shape[0]
    weights = [
        query_weight,
        key_weight,
        value_weight,
        gate_weight,
        outer_weight,
        inner_weight,
        signal_weight,
    ]
    splits = []
    running = 0
    for weight in weights[:-1]:
        running = running + weight.shape[1]
        splits.append(running)
    joined = jnp.concatenate(weights, axis=1)
    empty = jnp.zeros((row_count, joined.shape[1]), jnp.float32)
    piece = lax.all_gather(tokens, "tp", axis=1, tiled=True)
    summed = empty
    piece_f = piece.astype(jnp.float32)
    normed_piece = (piece.astype(jnp.float32) * norm_gain).astype(jnp.bfloat16)
    raw = jnp.dot(normed_piece, joined, preferred_element_type=jnp.float32)
    squares = jnp.sum(piece_f * piece_f, axis=-1)
    scale = lax.rsqrt(squares / width + 1e-06)
    projected = (raw * scale[:, None]).astype(jnp.bfloat16)
    query, key, value, attn_gate, outer, inner, signal = jnp.split(projected, splits, axis=1)
    head_count = lambdas.shape[0]
    key_size = query_weight.shape[1] // (head_count * 2)
    value_size = value_weight.shape[1] // head_count
    score_scale = key_size ** (-0.5)
    own_index = lax.axis_index("sp")
    local_pos = jnp.arange(row_count, dtype=jnp.int32)
    query_parts = [query]
    position_parts = [own_index * row_count + local_pos]
    query_parts = [
        segment.reshape(segment.shape[0], head_count, 2, key_size) for segment in query_parts
    ]

    def absorb(current, query_rows, row_pos, key_block, value_block, key_pos):
        running_max, summed, accum = current
        score = (
            jnp.einsum("qhmd,khmd->hmqk", query_rows, key_block, preferred_element_type=jnp.float32)
            * score_scale
        )
        visible = row_pos[:, None] >= key_pos[None, :]
        masked = jnp.where(visible, score, -1e30)
        new_max = jnp.maximum(running_max, jnp.max(masked, axis=-1, keepdims=True))
        weights_now = jnp.where(visible, jnp.exp(masked - new_max), 0.0)
        factor = jnp.exp(running_max - new_max)
        summed = summed * factor + jnp.sum(weights_now, axis=-1, keepdims=True)
        accum = accum * factor + jnp.einsum(
            "hmqk,khd->hmqd",
            weights_now.astype(jnp.bfloat16),
            value_block,
            preferred_element_type=jnp.float32,
        )
        return (new_max, summed, accum)

    def fresh(rows):
        return (
            jnp.full((head_count, 2, rows, 1), -1e30, jnp.float32),
            jnp.zeros((head_count, 2, rows, 1), jnp.float32),
            jnp.zeros((head_count, 2, rows, value_size), jnp.float32),
        )

    start_states = tuple((fresh(segment.shape[0]) for segment in query_parts))
    carry = start_states
    key_piece = lax.all_gather(key, "sp", axis=0, tiled=True)
    value_piece = lax.all_gather(value, "sp", axis=0, tiled=True)
    length = key_piece.shape[0]
    block_len = 512
    key_blocks = key_piece.reshape(length // block_len, block_len, head_count, 2, key_size)
    value_blocks = value_piece.reshape(length // block_len, block_len, head_count, value_size)

    def one_block(states, item):
        key_block, value_block, block_id = item
        first_key = block_id * block_len
        key_pos = first_key + jnp.arange(block_len, dtype=jnp.int32)
        updated = []
        for current, query_rows, row_pos in zip(states, query_parts, position_parts):

            def compute(held, query_rows=query_rows, row_pos=row_pos):
                return absorb(held, query_rows, row_pos, key_block, value_block, key_pos)

            def unchanged(held):
                return held

            updated.append(
                lax.cond(first_key <= row_pos[row_pos.shape[0] - 1], compute, unchanged, current)
            )
        return (tuple(updated), None)

    carry, _ = lax.scan(
        one_block,
        carry,
        (key_blocks, value_blocks, jnp.arange(length // block_len, dtype=jnp.int32)),
    )
    states = carry
    running_max = jnp.concatenate([held[0] for held in states], axis=2)
    summed = jnp.concatenate([held[1] for held in states], axis=2)
    accum = jnp.concatenate([held[2] for held in states], axis=2)
    mapped = accum / summed
    diff = mapped[:, 0] - lambdas[:, None, None] * mapped[:, 1]
    log_totals = jnp.log(summed[..., 0]) + running_max[..., 0]
    diff = jnp.transpose(diff, (1, 0, 2))
    normed = (
        diff
        * lax.rsqrt(jnp.mean(diff * diff, axis=-1, keepdims=True) + 1e-05)
        * head_gain.reshape(head_count, value_size)
    )
    normed = normed.reshape(row_count, head_count * value_size)
    head_out = (normed * jax.nn.silu(attn_gate.astype(jnp.float32))).astype(jnp.bfloat16)
    taps = conv_taps.shape[0]
    inner_sig = (inner.astype(jnp.float32) * signal.astype(jnp.float32)).astype(jnp.bfloat16)
    before = passed_along(inner_sig[row_count - (taps - 1) :], "sp", 1)
    extended = jnp.concatenate([before, inner_sig], axis=0).astype(jnp.float32)
    convolved = jnp.zeros((row_count, inner_sig.shape[1]), jnp.float32)
    for position in range(taps):
        convolved = convolved + conv_taps[position] * extended[position : position + row_count]
    conv_out = (outer.astype(jnp.float32) * convolved).astype(jnp.bfloat16)
    mixed = lax.psum_scatter(
        (
            jnp.dot(head_out, attn_out_weight, preferred_element_type=jnp.float32)
            + jnp.dot(conv_out, conv_out_weight, preferred_element_type=jnp.float32)
        ).astype(jnp.bfloat16),
        "tp",
        scatter_dimension=0,
        tiled=True,
    )
    return (mixed, log_totals)


RELAY = 4


def fused_kernel(
    sp_count,
    heads,
    tokens_ref,
    gain_ref,
    wq_hbm,
    wk_hbm,
    wv_hbm,
    wg_hbm,
    wouter_hbm,
    winner_hbm,
    wsignal_hbm,
    taps_ref,
    lambdas_ref,
    head_gain_ref,
    wo_hbm,
    wc_hbm,
    mixed_ref,
    totals_ref,
    other_tokens,
    normed,
    w_vmem,
    wo_vmem,
    wc_vmem,
    kv_send,
    q_send,
    kv_all,
    q_all,
    row_max,
    accum,
    gate,
    outer,
    inner_sig,
    tail_in,
    extended,
    conv_out,
    head_out,
    conv_part,
    o_send,
    o_all,
    lt_send,
    lt_all,
    part_send,
    part_recv,
    w_sem,
    tok_sem,
    tail_sem,
    part_sem,
    stage_s,
    stage_r,
    q_s,
    q_r,
    x_s,
    x_r,
    y_s,
    y_r,
    dx_s,
    dx_r,
    dy_s,
    dy_r,
    o_s,
    o_r,
    lt_s,
    lt_r,
    local_sem,
):
    rows, half = tokens_ref.shape
    width = 2 * half
    local = wq_hbm.shape[1]
    lanes = local // heads
    s = lax.axis_index("sp")
    t = lax.axis_index("tp")
    plane = s // RELAY
    member = lax.rem(s, RELAY)
    right_in_pair = member + 1 - 2 * lax.rem(member, 2)
    across = lax.rem(member + 2, RELAY)
    x_dev = plane * RELAY + right_in_pair
    y_dev = plane * RELAY + across
    following = lax.rem(s + 1, sp_count)
    preceding = lax.rem(s + sp_count - 1, sp_count)

    def at(sp_index, tp_index=None):
        return {"sp": sp_index, "tp": t if tp_index is None else tp_index}

    def remote(src, dst, send_sem, recv_sem, device):
        return pltpu.make_async_remote_copy(
            src_ref=src,
            dst_ref=dst,
            send_sem=send_sem,
            recv_sem=recv_sem,
            device_id=device,
            device_id_type=MESH,
        )

    sources = [wk_hbm, wv_hbm, wq_hbm, winner_hbm, wsignal_hbm, wouter_hbm, wg_hbm]
    weight_copies = [
        pltpu.make_async_copy(ref, w_vmem.at[i], w_sem.at[i]) for i, ref in enumerate(sources)
    ]
    weight_copies.append(pltpu.make_async_copy(wc_hbm, wc_vmem, w_sem.at[len(sources)]))
    weight_copies.append(pltpu.make_async_copy(wo_hbm, wo_vmem, w_sem.at[len(sources) + 1]))
    for copy in weight_copies:
        copy.start()

    barrier = pltpu.get_barrier_semaphore()
    greeted = [at(s, 1 - t), at(x_dev), at(y_dev), at(following), at(preceding)]
    for step in range(1, heads):
        greeted.append(at(lax.rem(plane + step, heads) * RELAY + member))
    for device in greeted:
        pl.semaphore_signal(barrier, inc=1, device_id=device, device_id_type=MESH)
    pl.semaphore_wait(barrier, len(greeted))

    tokens_out = remote(tokens_ref, other_tokens, tok_sem.at[0], tok_sem.at[1], at(s, 1 - t))
    tokens_out.start()

    row_max[...] = jnp.full(row_max.shape, -1e30, jnp.float32)
    accum[...] = jnp.zeros(accum.shape, jnp.float32)

    mine = pl.ds(pl.multiple_of(t * half, half), half)
    theirs = pl.ds(pl.multiple_of((1 - t) * half, half), half)
    own_f = tokens_ref[...].astype(jnp.float32)
    squares = jnp.sum(own_f * own_f, axis=-1, keepdims=True)
    normed[:, mine] = (own_f * gain_ref[:, mine]).astype(jnp.bfloat16)
    tokens_out.wait()
    other_f = other_tokens[...].astype(jnp.float32)
    squares = squares + jnp.sum(other_f * other_f, axis=-1, keepdims=True)
    normed[:, theirs] = (other_f * gain_ref[:, theirs]).astype(jnp.bfloat16)
    scale = lax.rsqrt(squares / width + 1e-06)

    def project(index):
        weight_copies[index].wait()
        raw = jnp.dot(normed[...], w_vmem[index], preferred_element_type=jnp.float32)
        return (raw * scale).astype(jnp.bfloat16)

    for index in range(2):
        projected = project(index)
        for h in range(heads):
            kv_send[h, :, index * lanes : (index + 1) * lanes] = projected[
                :, h * lanes : (h + 1) * lanes
            ]

    started = []

    def launch(copy):
        copy.start()
        started.append(copy)

    def block(plane_index, place):
        return kv_all.at[plane_index * RELAY + place]

    keep = pltpu.make_async_copy(kv_send.at[plane], kv_all.at[s], local_sem.at[0])
    keep.start()
    own_block = kv_send.at[plane]
    launch(remote(own_block, kv_all.at[s], x_s.at[0], x_r.at[plane], at(x_dev)))
    launch(remote(own_block, kv_all.at[s], y_s.at[0], y_r.at[plane], at(y_dev)))
    for step in range(1, heads):
        target = lax.rem(plane + step, heads)
        launch(
            remote(
                kv_send.at[target],
                kv_all.at[s],
                stage_s.at[step],
                stage_r.at[plane],
                at(target * RELAY + member),
            )
        )

    projected = project(2)
    for h in range(heads):
        q_send[h] = projected[:, h * lanes : (h + 1) * lanes]
    keep_q = pltpu.make_async_copy(q_send.at[plane], q_all.at[plane], local_sem.at[1])
    keep_q.start()
    q_copies = []
    for step in range(1, heads):
        target = lax.rem(plane + step, heads)
        q_copy = remote(
            q_send.at[target],
            q_all.at[plane],
            q_s.at[step],
            q_r.at[plane],
            at(target * RELAY + member),
        )
        launch(q_copy)

    inner = project(3).astype(jnp.float32)
    signal = project(4).astype(jnp.float32)
    inner_sig[...] = (inner * signal).astype(jnp.bfloat16)
    tail = tail_in.shape[0]
    launch(
        remote(
            inner_sig.at[pl.ds(rows - tail, tail)],
            tail_in,
            tail_sem.at[0],
            tail_sem.at[1],
            at(following),
        )
    )

    order = [plane] + [k + jnp.where(plane <= k, 1, 0) for k in range(heads - 1)]
    half_rows = rows // 2
    first_half, second_half = pl.ds(0, half_rows), pl.ds(half_rows, half_rows)

    def arrived(dst, recv_sem):
        remote(dst, dst, stage_s.at[0], recv_sem, at(x_dev)).wait_recv()

    def forward_stage(k):
        c = order[k]
        here = block(c, member)
        arrived(here, stage_r.at[c])
        launch(remote(here, here, x_s.at[k], x_r.at[c], at(x_dev)))
        launch(remote(here, here, y_s.at[k], y_r.at[c], at(y_dev)))

    def forward_square(k):
        c = order[k]
        from_x = block(c, right_in_pair)
        arrived(from_x, x_r.at[c])
        piece = from_x.at[first_half]
        launch(remote(piece, piece, dy_s.at[k], dy_r.at[c], at(y_dev)))
        from_y = block(c, across)
        arrived(from_y, y_r.at[c])
        piece = from_y.at[second_half]
        launch(remote(piece, piece, dx_s.at[k], dx_r.at[c], at(x_dev)))

    def finish_plane(k):
        c = order[k]
        diagonal = block(c, RELAY - 1 - member)
        arrived(diagonal.at[first_half], dy_r.at[c])
        arrived(diagonal.at[second_half], dx_r.at[c])

    exponent = (lanes // 2) ** (-0.5) * math.log2(math.e)
    span = RELAY * rows
    lane = lax.broadcasted_iota(jnp.int32, (1, lanes), 1)

    def attend(qi, c, masked):
        held = kv_all[pl.ds(c * RELAY, RELAY)].reshape(span, 2 * lanes)
        keys = held[:, :lanes]
        values = jnp.concatenate(
            [held[:, lanes:], jnp.ones((span, lanes), jnp.bfloat16)], axis=1
        )
        both = q_all[qi]
        for m in range(2):
            of_map = (lane < lanes // 2) if m == 0 else (lane >= lanes // 2)
            query = both * of_map.astype(jnp.float32).astype(jnp.bfloat16)
            score = (
                lax.dot_general(
                    query, keys, (((1,), (1,)), ((), ())), preferred_element_type=jnp.float32
                )
                * exponent
            )
            if masked:
                row = lax.broadcasted_iota(jnp.int32, (rows, span), 0) + member * rows
                col = lax.broadcasted_iota(jnp.int32, (rows, span), 1)
                score = jnp.where(row >= col, score, -1e30)
            before = row_max[2 * qi + m]
            top = jnp.maximum(before, jnp.max(score, axis=-1, keepdims=True))
            weights = jnp.exp2(score - top[:, :1]).astype(jnp.bfloat16)
            factor = jnp.exp2(before - top)[:, :1]
            row_max[2 * qi + m] = top
            accum[2 * qi + m] = accum[2 * qi + m] * factor + jnp.dot(
                weights, values, preferred_element_type=jnp.float32
            )

    def attend_plane(k):
        c = order[k]
        attend(c, c, True)

        for qi in range(1, heads):

            @pl.when(qi > c)
            def _(qi=qi):
                attend(qi, c, False)

    forward_stage(1)
    forward_square(0)
    outer[...] = project(5)
    gate[...] = project(6)

    arrived(tail_in, tail_sem.at[1])
    lead = extended.shape[0] - rows
    before_rows = tail_in[tail - lead :, :].astype(jnp.float32)
    extended[0:lead, :] = jnp.where(s > 0, before_rows, 0.0)
    extended[lead:, :] = inner_sig[...].astype(jnp.float32)
    tap_count = taps_ref.shape[0]
    convolved = jnp.zeros((rows, local), jnp.float32)
    for position in range(tap_count):
        offset = lead - (tap_count - 1) + position
        convolved = convolved + taps_ref[position : position + 1, :] * extended[
            offset : offset + rows, :
        ]
    conv_out[...] = (outer[...].astype(jnp.float32) * convolved).astype(jnp.bfloat16)

    keep.wait()
    keep_q.wait()
    for k in range(1, heads):
        c = order[k]
        arrived(q_all.at[c], q_r.at[c])
    for k in range(heads):
        if k + 2 < heads:
            forward_stage(k + 2)
        if k + 1 < heads:
            forward_square(k + 1)
        finish_plane(k)
        attend_plane(k)
        if k == 0:
            weight_copies[len(sources)].wait()
            conv_part[...] = jnp.dot(
                conv_out[...], wc_vmem[...], preferred_element_type=jnp.float32
            )

    lam = lambdas_ref[plane]
    own_gain = head_gain_ref[:, pl.ds(pl.multiple_of(plane * lanes, lanes), lanes)]
    column = lax.broadcasted_iota(jnp.int32, (rows, lanes), 1)
    keep_o = pltpu.make_async_copy(o_send.at[plane], o_all.at[plane], local_sem.at[2])
    keep_lt = pltpu.make_async_copy(lt_send.at[plane], lt_all.at[plane], local_sem.at[3])
    for step in list(range(1, heads)) + [0]:
        target = lax.rem(plane + step, heads)
        maps = []
        logs = []
        for m in range(2):
            held = accum[2 * target + m]
            total = held[:, lanes:]
            maps.append(held[:, :lanes] / total)
            logs.append(jnp.log(total) + row_max[2 * target + m] * math.log(2.0))
        diff = maps[0] - lam * maps[1]
        mean = jnp.mean(diff * diff, axis=-1, keepdims=True)
        o_send[target] = (diff * lax.rsqrt(mean + 1e-05) * own_gain).astype(jnp.bfloat16)
        turned = jnp.where(column == 0, logs[0], logs[1]).T
        lt_send[target] = turned[: lt_send.shape[1], :]
        if step == 0:
            keep_o.start()
            keep_lt.start()
        else:
            device = at(target * RELAY + member)
            launch(remote(o_send.at[target], o_all.at[plane], o_s.at[step], o_r.at[plane], device))
            launch(
                remote(lt_send.at[target], lt_all.at[plane], lt_s.at[step], lt_r.at[plane], device)
            )
    keep_o.wait()
    keep_lt.wait()
    for step in range(1, heads):
        source = lax.rem(plane + step, heads)
        arrived(o_all.at[source], o_r.at[source])
        arrived(lt_all.at[source], lt_r.at[source])
    for h in range(heads):
        totals_ref[h] = lt_all[h, 0:2, :]
        part = slice(h * lanes, (h + 1) * lanes)
        opened = gate[:, part].astype(jnp.float32)
        opened = opened / (1.0 + jnp.exp(-opened))
        head_out[:, part] = (o_all[h].astype(jnp.float32) * opened).astype(jnp.bfloat16)
    weight_copies[len(sources) + 1].wait()

    def partial_rows(which):
        there = pl.ds(pl.multiple_of(which * half_rows, half_rows), half_rows)
        attn = jnp.dot(head_out[there, :], wo_vmem[...], preferred_element_type=jnp.float32)
        return (attn + conv_part[there, :]).astype(jnp.bfloat16)

    part_send[...] = partial_rows(1 - t)
    exchange = remote(part_send, part_recv, part_sem.at[0], part_sem.at[1], at(s, 1 - t))
    exchange.start()
    own_rows = partial_rows(t).astype(jnp.float32)
    exchange.wait()
    mixed_ref[...] = (own_rows + part_recv[...].astype(jnp.float32)).astype(jnp.bfloat16)
    for copy in started:
        copy.wait_send()


def fused(sp_count, *args):
    tokens, norm_gain, wq = args[0], args[1], args[2]
    lambdas, head_gain = args[10], args[11]
    rows, half = tokens.shape
    heads = lambdas.shape[0]
    local = wq.shape[1]
    lanes = local // heads
    out_width = args[12].shape[1]
    bf16, f32 = jnp.bfloat16, jnp.float32
    vmem = pl.BlockSpec(memory_space=pltpu.VMEM)
    hbm = pl.BlockSpec(memory_space=pl.ANY)
    dma = pltpu.SemaphoreType.DMA
    operands = list(args)
    operands[1] = norm_gain.reshape(1, -1)
    operands[11] = head_gain.reshape(1, -1)
    return pl.pallas_call(
        functools.partial(fused_kernel, sp_count, heads),
        out_shape=(
            jax.ShapeDtypeStruct((rows // 2, out_width), bf16),
            jax.ShapeDtypeStruct((heads, 2, rows), f32),
        ),
        in_specs=[vmem, vmem]
        + [hbm] * 7
        + [vmem, pl.BlockSpec(memory_space=pltpu.SMEM), vmem, hbm, hbm],
        out_specs=(vmem, vmem),
        scratch_shapes=[
            pltpu.VMEM((rows, half), bf16),
            pltpu.VMEM((rows, 2 * half), bf16),
            pltpu.VMEM((7,) + wq.shape, bf16),
            pltpu.VMEM(args[12].shape, bf16),
            pltpu.VMEM(args[13].shape, bf16),
            pltpu.VMEM((heads, rows, 2 * lanes), bf16),
            pltpu.VMEM((heads, rows, lanes), bf16),
            pltpu.VMEM((sp_count, rows, 2 * lanes), bf16),
            pltpu.VMEM((heads, rows, lanes), bf16),
            pltpu.VMEM((2 * heads, rows, lanes), f32),
            pltpu.VMEM((2 * heads, rows, 2 * lanes), f32),
            pltpu.VMEM((rows, local), bf16),
            pltpu.VMEM((rows, local), bf16),
            pltpu.VMEM((rows, local), bf16),
            pltpu.VMEM((16, local), bf16),
            pltpu.VMEM((rows + 8, local), f32),
            pltpu.VMEM((rows, local), bf16),
            pltpu.VMEM((rows, local), bf16),
            pltpu.VMEM((rows, out_width), f32),
            pltpu.VMEM((heads, rows, lanes), bf16),
            pltpu.VMEM((heads, rows, lanes), bf16),
            pltpu.VMEM((heads, 8, rows), f32),
            pltpu.VMEM((heads, 8, rows), f32),
            pltpu.VMEM((rows // 2, out_width), bf16),
            pltpu.VMEM((rows // 2, out_width), bf16),
            dma((9,)),
            dma((2,)),
            dma((2,)),
            dma((2,)),
        ]
        + [dma((heads,)) for _ in range(16)]
        + [dma((4,))],
        compiler_params=pltpu.CompilerParams(
            collective_id=0, has_side_effects=True, vmem_limit_bytes=60 * 1024 * 1024
        ),
    )(*operands)


def fits_square(mesh, heads, rows, key_columns, value_columns):
    return (
        mesh.shape["tp"] == 2
        and mesh.shape["sp"] == heads * RELAY
        and heads > 1
        and rows % 32 == 0
        and key_columns == value_columns == heads * 128
    )


def solution(mesh):
    placed = (
        P("sp", "tp"),
        P(),
        P(None, "tp"),
        P(None, "tp"),
        P(None, "tp"),
        P(None, "tp"),
        P(None, "tp"),
        P(None, "tp"),
        P(None, "tp"),
        P(None, "tp"),
        P("tp"),
        P("tp"),
        P("tp", None),
        P("tp", None),
    )

    def step(*args):
        heads = args[10].shape[0]
        if fits_square(mesh, heads, args[0].shape[0], args[2].shape[1], args[4].shape[1]):
            return fused(mesh.shape["sp"], *args)
        return per_device(*args)

    return jax.shard_map(
        step,
        mesh=mesh,
        in_specs=placed,
        out_specs=(P(("sp", "tp"), None), P("tp", None, "sp")),
        check_vma=False,
    )
```

profile of v0, /device:TPU:3, one launch (start us, length us, event | category | flops | bytes accessed | tf_op | source)
XLA Modules:
  0.0 60.3 jit_solution(3195156483517193412)
XLA Ops:
  0.6 56.5 %shard_map.149 = (bf16[128,2048]{1,0:T(8,128)(2,1)}, f32[4,2,256]{2,1,0:T(2,128)}) custom-call(bf16[256,1024]{1,0:T(8,128)(2,1)} %tokens_ref.1, f32[1,2048]{1,0:T(1,128)} %bitcast.2, bf16[2048,512]{1,0:T(8,128)(2,1)} %wq_hbm.1, bf16[2048,512]{1,0:T(8,128)(2,1)} %wk_hbm.1, bf16[2048,512]{1,0:T(8,128)(2,1)} %wv_hbm.1, bf16[2048,512]{1,0:T(8,128)(2,1)} %wg_hbm.1, ...), custom_call_target="tpu_custom_call" | custom-call | tf_op jit(solution)/shard_map/pallas_call | solution.py:552
  57.1 1.9 %copy.18 = bf16[128,2048]{1,0:T(8,128)(2,1)} copy(bf16[128,2048]{1,0:T(8,128)(2,1)} %get-tuple-element.4) | data formatting | bytes 1048576
  59.0 1.3 %copy.19 = f32[4,2,256]{2,1,0:T(2,128)} copy(f32[4,2,256]{2,1,0:T(2,128)} %get-tuple-element.5) | data formatting | bytes 16384
where the time goes:
time: 60.5 us; the launch traced here: 60.3 us
  Pallas kernels  56.5 us (93%)
  local copies, waits for them, and re-layouts  3.18 us (5%)
  between operations  0.64 us (1%)
    pallas_call x1, Pallas kernels, fused(): pl.pallas_call(functools.partial(fused_kernel, sp_count, heads), out_shap...  56.5 us
    unnamed x2, local copies, waits for them, and re-layouts  3.18 us

commit v1 on v0

--- a/solution.py
+++ b/solution.py
@@ -172,8 +172,8 @@
 def fused_kernel(
     sp_count,
     heads,
-    tokens_ref,
-    gain_ref,
+    tokens_hbm,
+    gain_hbm,
     wq_hbm,
     wk_hbm,
     wv_hbm,
@@ -181,14 +181,20 @@
     wouter_hbm,
     winner_hbm,
     wsignal_hbm,
-    taps_ref,
-    lambdas_ref,
-    head_gain_ref,
+    taps_hbm,
+    lambdas_hbm,
+    head_gain_hbm,
     wo_hbm,
     wc_hbm,
     mixed_ref,
     totals_ref,
+    own_tokens,
     other_tokens,
+    gain_ref,
+    taps_ref,
+    head_gain_ref,
+    lam_own,
+    lam_other,
     normed,
     w_vmem,
     wo_vmem,
@@ -199,7 +205,7 @@
     q_all,
     row_max,
     accum,
-    gate,
+    opened,
     outer,
     inner_sig,
     tail_in,
@@ -214,6 +220,7 @@
     part_send,
     part_recv,
     w_sem,
+    in_sem,
     tok_sem,
     tail_sem,
     part_sem,
@@ -223,32 +230,31 @@
     q_r,
     x_s,
     x_r,
-    y_s,
-    y_r,
-    dx_s,
-    dx_r,
-    dy_s,
-    dy_r,
+    c_s,
+    c_r,
+    d_s,
+    d_r,
     o_s,
     o_r,
     lt_s,
     lt_r,
-    local_sem,
+    pair_sem,
+    met_sem,
 ):
-    rows, half = tokens_ref.shape
+    rows, half = own_tokens.shape
     width = 2 * half
     local = wq_hbm.shape[1]
     lanes = local // heads
     s = lax.axis_index("sp")
     t = lax.axis_index("tp")
     plane = s // RELAY
-    member = lax.rem(s, RELAY)
-    right_in_pair = member + 1 - 2 * lax.rem(member, 2)
-    across = lax.rem(member + 2, RELAY)
-    x_dev = plane * RELAY + right_in_pair
-    y_dev = plane * RELAY + across
-    following = lax.rem(s + 1, sp_count)
-    preceding = lax.rem(s + sp_count - 1, sp_count)
+    place = lax.rem(s, RELAY)
+    y = place // 2
+    x = lax.rem(place, 2)
+    member = 2 * t + x
+    home = t == y
+    low = plane < heads // 2
+    last = sp_count - 1
 
     def at(sp_index, tp_index=None):
         return {"sp": sp_index, "tp": t if tp_index is None else tp_index}
@@ -263,7 +269,28 @@
             device_id_type=MESH,
         )
 
-    sources = [wk_hbm, wv_hbm, wq_hbm, winner_hbm, wsignal_hbm, wouter_hbm, wg_hbm]
+    def worker(j):
+        return at(j * RELAY + member, y)
+
+    x_sp = s + 1 - 2 * x
+    x_dev = at(x_sp)
+    c_dev = at(s, 1 - t)
+
+    small = [
+        pltpu.make_async_copy(ref, dst, in_sem.at[i])
+        for i, (ref, dst) in enumerate(
+            [
+                (tokens_hbm, own_tokens),
+                (gain_hbm, gain_ref),
+                (lambdas_hbm, lam_own),
+                (taps_hbm, taps_ref),
+                (head_gain_hbm, head_gain_ref),
+            ]
+        )
+    ]
+    for copy in small:
+        copy.start()
+    sources = [wq_hbm, wk_hbm, wv_hbm, winner_hbm, wsignal_hbm, wouter_hbm, wg_hbm]
     weight_copies = [
         pltpu.make_async_copy(ref, w_vmem.at[i], w_sem.at[i]) for i, ref in enumerate(sources)
     ]
@@ -273,22 +300,71 @@
         copy.start()
 
     barrier = pltpu.get_barrier_semaphore()
-    greeted = [at(s, 1 - t), at(x_dev), at(y_dev), at(following), at(preceding)]
+
+    def signal(sem, device):
+        pl.semaphore_signal(sem, inc=1, device_id=device, device_id_type=MESH)
+
+    def greet(sp_index):
+        signal(barrier, at(sp_index, 1))
+
+    @pl.when(t == 1)
+    def _():
+        signal(barrier, at(s, 0))
+
     for step in range(1, heads):
-        greeted.append(at(lax.rem(plane + step, heads) * RELAY + member))
-    for device in greeted:
-        pl.semaphore_signal(barrier, inc=1, device_id=device, device_id_type=MESH)
-    pl.semaphore_wait(barrier, len(greeted))
-
-    tokens_out = remote(tokens_ref, other_tokens, tok_sem.at[0], tok_sem.at[1], at(s, 1 - t))
+        greet(lax.rem(plane + step, heads) * RELAY + member)
+
+    @pl.when(t != y)
+    def _():
+        greet(plane * RELAY + member)
+
+    greet(x_sp)
+
+    @pl.when(s < last)
+    def _():
+        greet(s + 1)
+
+    @pl.when(s > 0)
+    def _():
+        greet(s - 1)
+
+    @pl.when(t == 0)
+    def _():
+        pl.semaphore_wait(barrier, 1)
+        signal(pair_sem, at(s, 1))
+
+    @pl.when(t == 1)
+    def _():
+        pl.semaphore_wait(pair_sem, 1)
+
+    greetings = (
+        2 * heads + 1 + 2 * jnp.where(s > 0, 1, 0) + 2 * jnp.where(s < last, 1, 0)
+    )
+
+    def meet():
+        @pl.when(t == 1)
+        def _():
+            pl.semaphore_wait(barrier, greetings)
+            signal(met_sem, at(s, 0))
+
+        @pl.when(t == 0)
+        def _():
+            pl.semaphore_wait(met_sem, 1)
+
+    small[0].wait()
+    tokens_out = remote(own_tokens, other_tokens, tok_sem.at[0], tok_sem.at[1], c_dev)
     tokens_out.start()
+    small[2].wait()
+    lam_out = remote(lam_own, lam_other, tok_sem.at[2], tok_sem.at[3], c_dev)
+    lam_out.start()
 
     row_max[...] = jnp.full(row_max.shape, -1e30, jnp.float32)
     accum[...] = jnp.zeros(accum.shape, jnp.float32)
 
+    small[1].wait()
     mine = pl.ds(pl.multiple_of(t * half, half), half)
     theirs = pl.ds(pl.multiple_of((1 - t) * half, half), half)
-    own_f = tokens_ref[...].astype(jnp.float32)
+    own_f = own_tokens[...].astype(jnp.float32)
     squares = jnp.sum(own_f * own_f, axis=-1, keepdims=True)
     normed[:, mine] = (own_f * gain_ref[:, mine]).astype(jnp.bfloat16)
     tokens_out.wait()
@@ -302,104 +378,137 @@
         raw = jnp.dot(normed[...], w_vmem[index], preferred_element_type=jnp.float32)
         return (raw * scale).astype(jnp.bfloat16)
 
+    started = []
+
+    def launch(copy):
+        copy.start()
+        started.append(copy)
+
+    def farthest_first(i):
+        down = heads - 1 - i
+        down = down - jnp.where(down <= plane, 1, 0)
+        up = i + jnp.where(i >= plane, 1, 0)
+        return jnp.where(low, down, up)
+
+    def q_copy(j):
+        return remote(q_send.at[j], q_all.at[plane], q_s.at[j], q_r.at[plane], worker(j))
+
+    def kv_copy(j):
+        return remote(kv_send.at[j], kv_all.at[s], stage_s.at[j], stage_r.at[plane], worker(j))
+
+    def send_all(copy_of):
+        @pl.when(t != y)
+        def _():
+            copy_of(plane).start()
+
+        for i in range(heads - 1):
+            copy_of(farthest_first(i)).start()
+
+    def drain_all(copy_of):
+        for i in range(heads - 1):
+            copy_of(farthest_first(i)).wait_send()
+
+        @pl.when(t != y)
+        def _():
+            copy_of(plane).wait_send()
+
+    projected = project(0)
+    for h in range(heads):
+        q_send[h] = projected[:, h * lanes : (h + 1) * lanes]
+
+    @pl.when(home)
+    def _():
+        q_all[plane] = q_send[plane]
+
+    @pl.when(plane >= heads // 2)
+    def _():
+        meet()
+        send_all(q_copy)
+
     for index in range(2):
-        projected = project(index)
+        projected = project(1 + index)
         for h in range(heads):
             kv_send[h, :, index * lanes : (index + 1) * lanes] = projected[
                 :, h * lanes : (h + 1) * lanes
             ]
 
-    started = []
-
-    def launch(copy):
-        copy.start()
-        started.append(copy)
-
-    def block(plane_index, place):
-        return kv_all.at[plane_index * RELAY + place]
-
-    keep = pltpu.make_async_copy(kv_send.at[plane], kv_all.at[s], local_sem.at[0])
-    keep.start()
-    own_block = kv_send.at[plane]
-    launch(remote(own_block, kv_all.at[s], x_s.at[0], x_r.at[plane], at(x_dev)))
-    launch(remote(own_block, kv_all.at[s], y_s.at[0], y_r.at[plane], at(y_dev)))
-    for step in range(1, heads):
-        target = lax.rem(plane + step, heads)
-        launch(
-            remote(
-                kv_send.at[target],
-                kv_all.at[s],
-                stage_s.at[step],
-                stage_r.at[plane],
-                at(target * RELAY + member),
-            )
-        )
-
-    projected = project(2)
-    for h in range(heads):
-        q_send[h] = projected[:, h * lanes : (h + 1) * lanes]
-    keep_q = pltpu.make_async_copy(q_send.at[plane], q_all.at[plane], local_sem.at[1])
-    keep_q.start()
-    q_copies = []
-    for step in range(1, heads):
-        target = lax.rem(plane + step, heads)
-        q_copy = remote(
-            q_send.at[target],
-            q_all.at[plane],
-            q_s.at[step],
-            q_r.at[plane],
-            at(target * RELAY + member),
-        )
-        launch(q_copy)
-
-    inner = project(3).astype(jnp.float32)
-    signal = project(4).astype(jnp.float32)
-    inner_sig[...] = (inner * signal).astype(jnp.bfloat16)
-    tail = tail_in.shape[0]
-    launch(
-        remote(
-            inner_sig.at[pl.ds(rows - tail, tail)],
-            tail_in,
-            tail_sem.at[0],
-            tail_sem.at[1],
-            at(following),
-        )
-    )
-
-    order = [plane] + [k + jnp.where(plane <= k, 1, 0) for k in range(heads - 1)]
-    half_rows = rows // 2
-    first_half, second_half = pl.ds(0, half_rows), pl.ds(half_rows, half_rows)
+    @pl.when(home)
+    def _():
+        kv_all[s] = kv_send[plane]
+
+    @pl.when(low)
+    def _():
+        meet()
+
+    send_all(kv_copy)
+
+    @pl.when(low)
+    def _():
+        send_all(q_copy)
+
+    order = [jnp.where(k <= plane, plane - k, k) for k in range(heads)]
+
+    def block(plane_index, which):
+        return kv_all.at[plane_index * RELAY + which]
 
     def arrived(dst, recv_sem):
-        remote(dst, dst, stage_s.at[0], recv_sem, at(x_dev)).wait_recv()
+        remote(dst, dst, stage_s.at[0], recv_sem, x_dev).wait_recv()
 
     def forward_stage(k):
         c = order[k]
         here = block(c, member)
-        arrived(here, stage_r.at[c])
-        launch(remote(here, here, x_s.at[k], x_r.at[c], at(x_dev)))
-        launch(remote(here, here, y_s.at[k], y_r.at[c], at(y_dev)))
+        if k == 0:
+
+            @pl.when(t != y)
+            def _():
+                arrived(here, stage_r.at[c])
+
+        else:
+            arrived(here, stage_r.at[c])
+        launch(remote(here, here, x_s.at[k], x_r.at[c], x_dev))
+        launch(remote(here, here, c_s.at[k], c_r.at[c], c_dev))
 
     def forward_square(k):
         c = order[k]
-        from_x = block(c, right_in_pair)
+        from_x = block(c, member + 1 - 2 * x)
         arrived(from_x, x_r.at[c])
-        piece = from_x.at[first_half]
-        launch(remote(piece, piece, dy_s.at[k], dy_r.at[c], at(y_dev)))
-        from_y = block(c, across)
-        arrived(from_y, y_r.at[c])
-        piece = from_y.at[second_half]
-        launch(remote(piece, piece, dx_s.at[k], dx_r.at[c], at(x_dev)))
+        launch(remote(from_x, from_x, d_s.at[k], d_r.at[c], c_dev))
 
     def finish_plane(k):
         c = order[k]
-        diagonal = block(c, RELAY - 1 - member)
-        arrived(diagonal.at[first_half], dy_r.at[c])
-        arrived(diagonal.at[second_half], dx_r.at[c])
+        arrived(block(c, lax.rem(member + 2, RELAY)), c_r.at[c])
+        arrived(block(c, RELAY - 1 - member), d_r.at[c])
+
+    inner = project(3).astype(jnp.float32)
+    signal_f = project(4).astype(jnp.float32)
+    inner_sig[...] = (inner * signal_f).astype(jnp.bfloat16)
+    tail = tail_in.shape[0]
+    tail_copy = remote(
+        inner_sig.at[pl.ds(rows - tail, tail)],
+        tail_in,
+        tail_sem.at[0],
+        tail_sem.at[1],
+        at(lax.rem(s + 1, sp_count)),
+    )
+
+    @pl.when(s < last)
+    def _():
+        tail_copy.start()
+
+    forward_stage(0)
+    small[4].wait()
+    outer[...] = project(5)
+    gate = project(6).astype(jnp.float32)
+    opened[...] = gate / (1.0 + jnp.exp(-gate)) * head_gain_ref[...]
+    forward_square(0)
 
     exponent = (lanes // 2) ** (-0.5) * math.log2(math.e)
     span = RELAY * rows
     lane = lax.broadcasted_iota(jnp.int32, (1, lanes), 1)
+    masks = [
+        of_map.astype(jnp.float32).astype(jnp.bfloat16)
+        for of_map in (lane < lanes // 2, lane >= lanes // 2)
+    ]
 
     def attend(qi, c, masked):
         held = kv_all[pl.ds(c * RELAY, RELAY)].reshape(span, 2 * lanes)
@@ -409,11 +518,12 @@
         )
         both = q_all[qi]
         for m in range(2):
-            of_map = (lane < lanes // 2) if m == 0 else (lane >= lanes // 2)
-            query = both * of_map.astype(jnp.float32).astype(jnp.bfloat16)
             score = (
                 lax.dot_general(
-                    query, keys, (((1,), (1,)), ((), ())), preferred_element_type=jnp.float32
+                    both * masks[m],
+                    keys,
+                    (((1,), (1,)), ((), ())),
+                    preferred_element_type=jnp.float32,
                 )
                 * exponent
             )
@@ -430,94 +540,117 @@
                 weights, values, preferred_element_type=jnp.float32
             )
 
-    def attend_plane(k):
+    lam_pick = lax.broadcasted_iota(jnp.int32, (1, heads), 1) == plane
+    lam_out.wait()
+    lam_row = jnp.where(home, lam_own[...], lam_other[...])
+    lam = jnp.sum(jnp.where(lam_pick, lam_row, 0.0), axis=-1, keepdims=True)
+    column = lax.broadcasted_iota(jnp.int32, (rows, lanes), 1)
+
+    def o_copy(q):
+        return remote(o_send.at[q], o_all.at[plane], o_s.at[q], o_r.at[plane], worker(q))
+
+    def lt_copy(q):
+        return remote(lt_send.at[q], lt_all.at[plane], lt_s.at[q], lt_r.at[plane], worker(q))
+
+    def finalize(q):
+        maps = []
+        logs = []
+        for m in range(2):
+            held = accum[2 * q + m]
+            total = held[:, lanes:]
+            maps.append(held[:, :lanes] / total)
+            logs.append(jnp.log(total) + row_max[2 * q + m] * math.log(2.0))
+        diff = maps[0] - lam * maps[1]
+        mean = jnp.mean(diff * diff, axis=-1, keepdims=True)
+        o_send[q] = (diff * lax.rsqrt(mean + 1e-05)).astype(jnp.bfloat16)
+        turned = jnp.where(column == 0, logs[0], logs[1]).T
+        lt_send[q] = turned[:2, :]
+        away = (q != plane) | (t != y)
+
+        @pl.when(away)
+        def _():
+            o_copy(q).start()
+            lt_copy(q).start()
+
+        @pl.when(jnp.logical_not(away))
+        def _():
+            o_all[plane] = o_send[q]
+            lt_all[plane] = lt_send[q]
+
+    def q_arrived(q):
+        @pl.when((q != plane) | (t != y))
+        def _():
+            arrived(q_all.at[q], q_r.at[q])
+
+    for k in range(heads):
         c = order[k]
+        if k + 1 < heads:
+            forward_stage(k + 1)
+        finish_plane(k)
+
+        @pl.loop(c + 1, heads)
+        def _(q, k=k, c=c):
+            if k == 0:
+                q_arrived(q)
+            attend(q, c, False)
+            if k > 0:
+
+                @pl.when((k == plane) & (q <= plane))
+                def _():
+                    finalize(q)
+
+        @pl.when(k <= plane)
+        def _(c=c):
+            q_arrived(c)
+
         attend(c, c, True)
 
-        for qi in range(1, heads):
-
-            @pl.when(qi > c)
-            def _(qi=qi):
-                attend(qi, c, False)
-
-    forward_stage(1)
-    forward_square(0)
-    outer[...] = project(5)
-    gate[...] = project(6)
-
-    arrived(tail_in, tail_sem.at[1])
-    lead = extended.shape[0] - rows
-    before_rows = tail_in[tail - lead :, :].astype(jnp.float32)
-    extended[0:lead, :] = jnp.where(s > 0, before_rows, 0.0)
-    extended[lead:, :] = inner_sig[...].astype(jnp.float32)
-    tap_count = taps_ref.shape[0]
-    convolved = jnp.zeros((rows, local), jnp.float32)
-    for position in range(tap_count):
-        offset = lead - (tap_count - 1) + position
-        convolved = convolved + taps_ref[position : position + 1, :] * extended[
-            offset : offset + rows, :
-        ]
-    conv_out[...] = (outer[...].astype(jnp.float32) * convolved).astype(jnp.bfloat16)
-
-    keep.wait()
-    keep_q.wait()
-    for k in range(1, heads):
-        c = order[k]
-        arrived(q_all.at[c], q_r.at[c])
-    for k in range(heads):
-        if k + 2 < heads:
-            forward_stage(k + 2)
+        @pl.when(k >= plane)
+        def _(c=c):
+            finalize(c)
+
         if k + 1 < heads:
             forward_square(k + 1)
-        finish_plane(k)
-        attend_plane(k)
         if k == 0:
+            small[3].wait()
+
+            @pl.when(s > 0)
+            def _():
+                arrived(tail_in, tail_sem.at[1])
+
+            @pl.when(s == 0)
+            def _():
+                tail_in[...] = jnp.zeros(tail_in.shape, jnp.bfloat16)
+
+            lead = extended.shape[0] - rows
+            extended[0:lead, :] = tail_in[tail - lead :, :].astype(jnp.float32)
+            extended[lead:, :] = inner_sig[...].astype(jnp.float32)
+            tap_count = taps_ref.shape[0]
+            convolved = jnp.zeros((rows, local), jnp.float32)
+            for position in range(tap_count):
+                offset = lead - (tap_count - 1) + position
+                convolved = convolved + taps_ref[position : position + 1, :] * extended[
+                    offset : offset + rows, :
+                ]
+            conv_out[...] = (outer[...].astype(jnp.float32) * convolved).astype(jnp.bfloat16)
             weight_copies[len(sources)].wait()
             conv_part[...] = jnp.dot(
                 conv_out[...], wc_vmem[...], preferred_element_type=jnp.float32
             )
 
-    lam = lambdas_ref[plane]
-    own_gain = head_gain_ref[:, pl.ds(pl.multiple_of(plane * lanes, lanes), lanes)]
-    column = lax.broadcasted_iota(jnp.int32, (rows, lanes), 1)
-    keep_o = pltpu.make_async_copy(o_send.at[plane], o_all.at[plane], local_sem.at[2])
-    keep_lt = pltpu.make_async_copy(lt_send.at[plane], lt_all.at[plane], local_sem.at[3])
-    for step in list(range(1, heads)) + [0]:
-        target = lax.rem(plane + step, heads)
-        maps = []
-        logs = []
-        for m in range(2):
-            held = accum[2 * target + m]
-            total = held[:, lanes:]
-            maps.append(held[:, :lanes] / total)
-            logs.append(jnp.log(total) + row_max[2 * target + m] * math.log(2.0))
-        diff = maps[0] - lam * maps[1]
-        mean = jnp.mean(diff * diff, axis=-1, keepdims=True)
-        o_send[target] = (diff * lax.rsqrt(mean + 1e-05) * own_gain).astype(jnp.bfloat16)
-        turned = jnp.where(column == 0, logs[0], logs[1]).T
-        lt_send[target] = turned[: lt_send.shape[1], :]
-        if step == 0:
-            keep_o.start()
-            keep_lt.start()
-        else:
-            device = at(target * RELAY + member)
-            launch(remote(o_send.at[target], o_all.at[plane], o_s.at[step], o_r.at[plane], device))
-            launch(
-                remote(lt_send.at[target], lt_all.at[plane], lt_s.at[step], lt_r.at[plane], device)
-            )
-    keep_o.wait()
-    keep_lt.wait()
-    for step in range(1, heads):
-        source = lax.rem(plane + step, heads)
-        arrived(o_all.at[source], o_r.at[source])
-        arrived(lt_all.at[source], lt_r.at[source])
+    weight_copies[len(sources) + 1].wait()
+    half_rows = rows // 2
+    for j in range(heads):
+
+        @pl.when((j != plane) | (t != y))
+        def _(j=j):
+            arrived(o_all.at[j], o_r.at[j])
+            arrived(lt_all.at[j], lt_r.at[j])
+
     for h in range(heads):
-        totals_ref[h] = lt_all[h, 0:2, :]
+        totals_ref[h] = lt_all[h]
         part = slice(h * lanes, (h + 1) * lanes)
-        opened = gate[:, part].astype(jnp.float32)
-        opened = opened / (1.0 + jnp.exp(-opened))
-        head_out[:, part] = (o_all[h].astype(jnp.float32) * opened).astype(jnp.bfloat16)
-    weight_copies[len(sources) + 1].wait()
+        head_out[:, part] = (o_all[h].astype(jnp.float32) * opened[:, part]).astype(jnp.bfloat16)
 
     def partial_rows(which):
         there = pl.ds(pl.multiple_of(which * half_rows, half_rows), half_rows)
@@ -525,13 +658,21 @@
         return (attn + conv_part[there, :]).astype(jnp.bfloat16)
 
     part_send[...] = partial_rows(1 - t)
-    exchange = remote(part_send, part_recv, part_sem.at[0], part_sem.at[1], at(s, 1 - t))
+    exchange = remote(part_send, part_recv, part_sem.at[0], part_sem.at[1], c_dev)
     exchange.start()
     own_rows = partial_rows(t).astype(jnp.float32)
     exchange.wait()
     mixed_ref[...] = (own_rows + part_recv[...].astype(jnp.float32)).astype(jnp.bfloat16)
     for copy in started:
         copy.wait_send()
+    drain_all(q_copy)
+    drain_all(kv_copy)
+    drain_all(o_copy)
+    drain_all(lt_copy)
+
+    @pl.when(s < last)
+    def _():
+        tail_copy.wait_send()
 
 
 def fused(sp_count, *args):
@@ -548,6 +689,7 @@
     dma = pltpu.SemaphoreType.DMA
     operands = list(args)
     operands[1] = norm_gain.reshape(1, -1)
+    operands[10] = lambdas.reshape(1, -1)
     operands[11] = head_gain.reshape(1, -1)
     return pl.pallas_call(
         functools.partial(fused_kernel, sp_count, heads),
@@ -555,12 +697,16 @@
             jax.ShapeDtypeStruct((rows // 2, out_width), bf16),
             jax.ShapeDtypeStruct((heads, 2, rows), f32),
         ),
-        in_specs=[vmem, vmem]
-        + [hbm] * 7
-        + [vmem, pl.BlockSpec(memory_space=pltpu.SMEM), vmem, hbm, hbm],
+        in_specs=[hbm] * len(operands),
         out_specs=(vmem, vmem),
         scratch_shapes=[
             pltpu.VMEM((rows, half), bf16),
+            pltpu.VMEM((rows, half), bf16),
+            pltpu.VMEM((1, 2 * half), f32),
+            pltpu.VMEM(args[9].shape, f32),
+            pltpu.VMEM((1, local), f32),
+            pltpu.VMEM((1, heads), f32),
+            pltpu.VMEM((1, heads), f32),
             pltpu.VMEM((rows, 2 * half), bf16),
             pltpu.VMEM((7,) + wq.shape, bf16),
             pltpu.VMEM(args[12].shape, bf16),
@@ -571,7 +717,7 @@
             pltpu.VMEM((heads, rows, lanes), bf16),
             pltpu.VMEM((2 * heads, rows, lanes), f32),
             pltpu.VMEM((2 * heads, rows, 2 * lanes), f32),
-            pltpu.VMEM((rows, local), bf16),
+            pltpu.VMEM((rows, local), f32),
             pltpu.VMEM((rows, local), bf16),
             pltpu.VMEM((rows, local), bf16),
             pltpu.VMEM((16, local), bf16),
@@ -581,17 +727,18 @@
             pltpu.VMEM((rows, out_width), f32),
             pltpu.VMEM((heads, rows, lanes), bf16),
             pltpu.VMEM((heads, rows, lanes), bf16),
-            pltpu.VMEM((heads, 8, rows), f32),
-            pltpu.VMEM((heads, 8, rows), f32),
+            pltpu.VMEM((heads, 2, rows), f32),
+            pltpu.VMEM((heads, 2, rows), f32),
             pltpu.VMEM((rows // 2, out_width), bf16),
             pltpu.VMEM((rows // 2, out_width), bf16),
             dma((9,)),
-            dma((2,)),
+            dma((5,)),
+            dma((4,)),
             dma((2,)),
             dma((2,)),
         ]
-        + [dma((heads,)) for _ in range(16)]
-        + [dma((4,))],
+        + [dma((heads,)) for _ in range(14)]
+        + [pltpu.SemaphoreType.REGULAR, pltpu.SemaphoreType.REGULAR],
         compiler_params=pltpu.CompilerParams(
             collective_id=0, has_side_effects=True, vmem_limit_bytes=60 * 1024 * 1024
         ),

time: 60.5 us -> 56.9 us (0.940)
  the two profiles are of different devices: /device:TPU:3 before, /device:TPU:0 now
where the time goes in v1:
time: 56.9 us; the launch traced here: 56.7 us
  Pallas kernels  52.9 us (93%)
  local copies, waits for them, and re-layouts  3.18 us (6%)
  between operations  0.64 us (1%)
    pallas_call x1, Pallas kernels, fused(): pl.pallas_call(functools.partial(fused_kernel, sp_count, heads), out_shap...  52.9 us
    unnamed x2, local copies, waits for them, and re-layouts  3.18 us

profile of v1, /device:TPU:0, one launch (start us, length us, event | category | flops | bytes accessed | tf_op | source)
XLA Modules:
  0.0 56.7 jit_solution(14033806344195191653)
XLA Ops:
  0.6 52.9 %shard_map.149 = (bf16[128,2048]{1,0:T(8,128)(2,1)}, f32[4,2,256]{2,1,0:T(2,128)}) custom-call(bf16[256,1024]{1,0:T(8,128)(2,1)} %tokens_hbm.1, f32[1,2048]{1,0:T(1,128)} %bitcast.3, bf16[2048,512]{1,0:T(8,128)(2,1)} %wq_hbm.1, bf16[2048,512]{1,0:T(8,128)(2,1)} %wk_hbm.1, bf16[2048,512]{1,0:T(8,128)(2,1)} %wv_hbm.1, bf16[2048,512]{1,0:T(8,128)(2,1)} %wg_hbm.1, ...), custom_call_target="tpu_custom_call" | custom-call | tf_op jit(solution)/shard_map/pallas_call | solution.py:694
  53.5 1.9 %copy.18 = bf16[128,2048]{1,0:T(8,128)(2,1)} copy(bf16[128,2048]{1,0:T(8,128)(2,1)} %get-tuple-element.4) | data formatting | bytes 1048576
  55.4 1.3 %copy.19 = f32[4,2,256]{2,1,0:T(2,128)} copy(f32[4,2,256]{2,1,0:T(2,128)} %get-tuple-element.5) | data formatting | bytes 16384

commit v2 on v1

--- a/solution.py
+++ b/solution.py
@@ -296,8 +296,7 @@
     ]
     weight_copies.append(pltpu.make_async_copy(wc_hbm, wc_vmem, w_sem.at[len(sources)]))
     weight_copies.append(pltpu.make_async_copy(wo_hbm, wo_vmem, w_sem.at[len(sources) + 1]))
-    for copy in weight_copies:
-        copy.start()
+    weight_copies[0].start()
 
     barrier = pltpu.get_barrier_semaphore()
 
@@ -354,6 +353,8 @@
     small[0].wait()
     tokens_out = remote(own_tokens, other_tokens, tok_sem.at[0], tok_sem.at[1], c_dev)
     tokens_out.start()
+    for copy in weight_copies[1:]:
+        copy.start()
     small[2].wait()
     lam_out = remote(lam_own, lam_other, tok_sem.at[2], tok_sem.at[3], c_dev)
     lam_out.start()
@@ -373,22 +374,15 @@
     normed[:, theirs] = (other_f * gain_ref[:, theirs]).astype(jnp.bfloat16)
     scale = lax.rsqrt(squares / width + 1e-06)
 
-    def project(index):
+    def project(index, scale=scale):
         weight_copies[index].wait()
         raw = jnp.dot(normed[...], w_vmem[index], preferred_element_type=jnp.float32)
         return (raw * scale).astype(jnp.bfloat16)
 
-    started = []
-
-    def launch(copy):
-        copy.start()
-        started.append(copy)
-
-    def farthest_first(i):
-        down = heads - 1 - i
-        down = down - jnp.where(down <= plane, 1, 0)
-        up = i + jnp.where(i >= plane, 1, 0)
-        return jnp.where(low, down, up)
+    def nearest_first(i):
+        rising = jnp.where(i < plane, plane - 1 - i, i + 1)
+        falling = jnp.where(i < heads - 1 - plane, plane + 1 + i, heads - 2 - i)
+        return jnp.where(low, falling, rising)
 
     def q_copy(j):
         return remote(q_send.at[j], q_all.at[plane], q_s.at[j], q_r.at[plane], worker(j))
@@ -402,17 +396,18 @@
             copy_of(plane).start()
 
         for i in range(heads - 1):
-            copy_of(farthest_first(i)).start()
+            copy_of(nearest_first(i)).start()
 
     def drain_all(copy_of):
         for i in range(heads - 1):
-            copy_of(farthest_first(i)).wait_send()
+            copy_of(nearest_first(i)).wait_send()
 
         @pl.when(t != y)
         def _():
             copy_of(plane).wait_send()
 
-    projected = project(0)
+    exponent = (lanes // 2) ** (-0.5) * math.log2(math.e)
+    projected = project(0, scale * exponent)
     for h in range(heads):
         q_send[h] = projected[:, h * lanes : (h + 1) * lanes]
 
@@ -446,7 +441,8 @@
     def _():
         send_all(q_copy)
 
-    order = [jnp.where(k <= plane, plane - k, k) for k in range(heads)]
+    def order(k):
+        return jnp.where(k <= plane, plane - k, k)
 
     def block(plane_index, which):
         return kv_all.at[plane_index * RELAY + which]
@@ -454,30 +450,35 @@
     def arrived(dst, recv_sem):
         remote(dst, dst, stage_s.at[0], recv_sem, x_dev).wait_recv()
 
+    def along_x(k):
+        here = block(order(k), member)
+        return remote(here, here, x_s.at[k], x_r.at[order(k)], x_dev)
+
+    def across(k):
+        here = block(order(k), member)
+        return remote(here, here, c_s.at[k], c_r.at[order(k)], c_dev)
+
+    def onward(k):
+        from_x = block(order(k), member + 1 - 2 * x)
+        return remote(from_x, from_x, d_s.at[k], d_r.at[order(k)], c_dev)
+
     def forward_stage(k):
-        c = order[k]
-        here = block(c, member)
-        if k == 0:
-
-            @pl.when(t != y)
-            def _():
-                arrived(here, stage_r.at[c])
-
-        else:
-            arrived(here, stage_r.at[c])
-        launch(remote(here, here, x_s.at[k], x_r.at[c], x_dev))
-        launch(remote(here, here, c_s.at[k], c_r.at[c], c_dev))
+        along_x(k).start()
+        across(k).start()
 
     def forward_square(k):
-        c = order[k]
-        from_x = block(c, member + 1 - 2 * x)
-        arrived(from_x, x_r.at[c])
-        launch(remote(from_x, from_x, d_s.at[k], d_r.at[c], c_dev))
+        c = order(k)
+        arrived(block(c, member + 1 - 2 * x), x_r.at[c])
+        onward(k).start()
 
     def finish_plane(k):
-        c = order[k]
+        c = order(k)
         arrived(block(c, lax.rem(member + 2, RELAY)), c_r.at[c])
         arrived(block(c, RELAY - 1 - member), d_r.at[c])
+
+    @pl.when(home)
+    def _():
+        forward_stage(0)
 
     inner = project(3).astype(jnp.float32)
     signal_f = project(4).astype(jnp.float32)
@@ -495,14 +496,17 @@
     def _():
         tail_copy.start()
 
-    forward_stage(0)
+    @pl.when(t != y)
+    def _():
+        arrived(block(plane, member), stage_r.at[plane])
+        forward_stage(0)
+
     small[4].wait()
     outer[...] = project(5)
     gate = project(6).astype(jnp.float32)
     opened[...] = gate / (1.0 + jnp.exp(-gate)) * head_gain_ref[...]
     forward_square(0)
 
-    exponent = (lanes // 2) ** (-0.5) * math.log2(math.e)
     span = RELAY * rows
     lane = lax.broadcasted_iota(jnp.int32, (1, lanes), 1)
     masks = [
@@ -510,35 +514,43 @@
         for of_map in (lane < lanes // 2, lane >= lanes // 2)
     ]
 
-    def attend(qi, c, masked):
-        held = kv_all[pl.ds(c * RELAY, RELAY)].reshape(span, 2 * lanes)
+    def attend_plane(c):
+        held = kv_all[c * RELAY : (c + 1) * RELAY].reshape(span, 2 * lanes)
         keys = held[:, :lanes]
         values = jnp.concatenate(
             [held[:, lanes:], jnp.ones((span, lanes), jnp.bfloat16)], axis=1
         )
-        both = q_all[qi]
-        for m in range(2):
-            score = (
-                lax.dot_general(
-                    both * masks[m],
-                    keys,
-                    (((1,), (1,)), ((), ())),
-                    preferred_element_type=jnp.float32,
-                )
-                * exponent
+
+        def scores(qi, m):
+            score = lax.dot_general(
+                q_all[qi] * masks[m],
+                keys,
+                (((1,), (1,)), ((), ())),
+                preferred_element_type=jnp.float32,
             )
-            if masked:
+            if qi == c:
                 row = lax.broadcasted_iota(jnp.int32, (rows, span), 0) + member * rows
                 col = lax.broadcasted_iota(jnp.int32, (rows, span), 1)
                 score = jnp.where(row >= col, score, -1e30)
-            before = row_max[2 * qi + m]
+            return score
+
+        def absorb(at_row, score):
+            before = row_max[at_row]
             top = jnp.maximum(before, jnp.max(score, axis=-1, keepdims=True))
             weights = jnp.exp2(score - top[:, :1]).astype(jnp.bfloat16)
-            factor = jnp.exp2(before - top)[:, :1]
-            row_max[2 * qi + m] = top
-            accum[2 * qi + m] = accum[2 * qi + m] * factor + jnp.dot(
-                weights, values, preferred_element_type=jnp.float32
-            )
+            factor = jnp.exp2(before - top)
+            row_max[at_row] = top
+            update = jnp.dot(weights, values, preferred_element_type=jnp.float32)
+            for part in (slice(0, lanes), slice(lanes, 2 * lanes)):
+                accum[at_row, :, part] = accum[at_row, :, part] * factor + update[:, part]
+
+        items = [(qi, m) for qi in range(heads - 1, c - 1, -1) for m in range(2)]
+        upcoming = scores(*items[0])
+        for i, (qi, m) in enumerate(items):
+            score = upcoming
+            if i + 1 < len(items):
+                upcoming = scores(*items[i + 1])
+            absorb(2 * qi + m, score)
 
     lam_pick = lax.broadcasted_iota(jnp.int32, (1, heads), 1) == plane
     lam_out.wait()
@@ -582,61 +594,69 @@
         def _():
             arrived(q_all.at[q], q_r.at[q])
 
-    for k in range(heads):
-        c = order[k]
-        if k + 1 < heads:
+    def convolve():
+        small[3].wait()
+
+        @pl.when(s > 0)
+        def _():
+            arrived(tail_in, tail_sem.at[1])
+
+        @pl.when(s == 0)
+        def _():
+            tail_in[...] = jnp.zeros(tail_in.shape, jnp.bfloat16)
+
+        lead = extended.shape[0] - rows
+        extended[0:lead, :] = tail_in[tail - lead :, :].astype(jnp.float32)
+        extended[lead:, :] = inner_sig[...].astype(jnp.float32)
+        tap_count = taps_ref.shape[0]
+        convolved = jnp.zeros((rows, local), jnp.float32)
+        for position in range(tap_count):
+            offset = lead - (tap_count - 1) + position
+            convolved = convolved + taps_ref[position : position + 1, :] * extended[
+                offset : offset + rows, :
+            ]
+        conv_out[...] = (outer[...].astype(jnp.float32) * convolved).astype(jnp.bfloat16)
+        weight_copies[len(sources)].wait()
+        conv_part[...] = jnp.dot(
+            conv_out[...], wc_vmem[...], preferred_element_type=jnp.float32
+        )
+
+    @pl.loop(0, heads)
+    def _(k):
+        c = order(k)
+
+        @pl.when(k + 1 < heads)
+        def _():
+            following = order(k + 1)
+            arrived(block(following, member), stage_r.at[following])
             forward_stage(k + 1)
+
+        @pl.loop(c, heads)
+        def _(q):
+            @pl.when((k == 0) | ((q == c) & (k <= plane)))
+            def _():
+                q_arrived(q)
+
         finish_plane(k)
-
-        @pl.loop(c + 1, heads)
-        def _(q, k=k, c=c):
-            if k == 0:
-                q_arrived(q)
-            attend(q, c, False)
-            if k > 0:
-
-                @pl.when((k == plane) & (q <= plane))
-                def _():
-                    finalize(q)
-
-        @pl.when(k <= plane)
-        def _(c=c):
-            q_arrived(c)
-
-        attend(c, c, True)
-
-        @pl.when(k >= plane)
-        def _(c=c):
-            finalize(c)
-
-        if k + 1 < heads:
+        for cc in range(heads):
+
+            @pl.when(c == cc)
+            def _(cc=cc):
+                attend_plane(cc)
+
+        @pl.when(k + 1 < heads)
+        def _():
             forward_square(k + 1)
-        if k == 0:
-            small[3].wait()
-
-            @pl.when(s > 0)
+
+        @pl.loop(0, heads)
+        def _(q):
+            @pl.when(((k == plane) & (q <= plane)) | ((k > plane) & (q == c)))
             def _():
-                arrived(tail_in, tail_sem.at[1])
-
-            @pl.when(s == 0)
-            def _():
-                tail_in[...] = jnp.zeros(tail_in.shape, jnp.bfloat16)
-
-            lead = extended.shape[0] - rows
-            extended[0:lead, :] = tail_in[tail - lead :, :].astype(jnp.float32)
-            extended[lead:, :] = inner_sig[...].astype(jnp.float32)
-            tap_count = taps_ref.shape[0]
-            convolved = jnp.zeros((rows, local), jnp.float32)
-            for position in range(tap_count):
-                offset = lead - (tap_count - 1) + position
-                convolved = convolved + taps_ref[position : position + 1, :] * extended[
-                    offset : offset + rows, :
-                ]
-            conv_out[...] = (outer[...].astype(jnp.float32) * convolved).astype(jnp.bfloat16)
-            weight_copies[len(sources)].wait()
-            conv_part[...] = jnp.dot(
-                conv_out[...], wc_vmem[...], preferred_element_type=jnp.float32
-            )
+                finalize(q)
+
+        @pl.when(k == 0)
+        def _():
+            convolve()
 
     weight_copies[len(sources) + 1].wait()
     half_rows = rows // 2
@@ -663,8 +683,10 @@
     own_rows = partial_rows(t).astype(jnp.float32)
     exchange.wait()
     mixed_ref[...] = (own_rows + part_recv[...].astype(jnp.float32)).astype(jnp.bfloat16)
-    for copy in started:
-        copy.wait_send()
+    for k in range(heads):
+        along_x(k).wait_send()
+        across(k).wait_send()
+        onward(k).wait_send()
     drain_all(q_copy)
     drain_all(kv_copy)
     drain_all(o_copy)

time: 56.9 us -> 52.5 us (0.923)
  Pallas kernels: 52.9 us -> 48.5 us
    pallas_call x1, Pallas kernels: 52.9 us -> 48.5 us  [fused(): pl.pallas_call(functools.partial(fused_kernel, sp_count, heads), out_shap...]
where the time goes in v2:
time: 52.5 us; the launch traced here: 52.3 us
  Pallas kernels  48.5 us (92%)
  local copies, waits for them, and re-layouts  3.18 us (6%)
  between operations  0.64 us (1%)
    pallas_call x1, Pallas kernels, fused(): pl.pallas_call(functools.partial(fused_kernel, sp_count, heads), out_shap...  48.5 us
    unnamed x2, local copies, waits for them, and re-layouts  3.18 us

profile of v2, /device:TPU:0, one launch (start us, length us, event | category | flops | bytes accessed | tf_op | source)
XLA Modules:
  0.0 52.3 jit_solution(10373555934467822929)
XLA Ops:
  0.6 48.5 %shard_map.149 = (bf16[128,2048]{1,0:T(8,128)(2,1)}, f32[4,2,256]{2,1,0:T(2,128)}) custom-call(bf16[256,1024]{1,0:T(8,128)(2,1)} %tokens_hbm.1, f32[1,2048]{1,0:T(1,128)} %bitcast.3, bf16[2048,512]{1,0:T(8,128)(2,1)} %wq_hbm.1, bf16[2048,512]{1,0:T(8,128)(2,1)} %wk_hbm.1, bf16[2048,512]{1,0:T(8,128)(2,1)} %wv_hbm.1, bf16[2048,512]{1,0:T(8,128)(2,1)} %wg_hbm.1, ...), custom_call_target="tpu_custom_call" | custom-call | tf_op jit(solution)/shard_map/pallas_call | solution.py:716
  49.1 1.9 %copy.18 = bf16[128,2048]{1,0:T(8,128)(2,1)} copy(bf16[128,2048]{1,0:T(8,128)(2,1)} %get-tuple-element.4) | data formatting | bytes 1048576
  51.0 1.3 %copy.19 = f32[4,2,256]{2,1,0:T(2,128)} copy(f32[4,2,256]{2,1,0:T(2,128)} %get-tuple-element.5) | data formatting | bytes 16384

commit v3 on v2

--- a/solution.py
+++ b/solution.py
@@ -217,6 +217,10 @@
     o_all,
     lt_send,
     lt_all,
+    p_send,
+    p_all,
+    pl_send,
+    pl_all,
     part_send,
     part_recv,
     w_sem,
@@ -238,6 +242,10 @@
     o_r,
     lt_s,
     lt_r,
+    p_s,
+    p_r,
+    pl_s,
+    pl_r,
     pair_sem,
     met_sem,
 ):
@@ -254,6 +262,8 @@
     member = 2 * t + x
     home = t == y
     low = plane < heads // 2
+    high = plane >= heads // 2
+    mirror = heads - 1 - plane
     last = sp_count - 1
 
     def at(sp_index, tp_index=None):
@@ -290,7 +300,7 @@
     ]
     for copy in small:
         copy.start()
-    sources = [wq_hbm, wk_hbm, wv_hbm, winner_hbm, wsignal_hbm, wouter_hbm, wg_hbm]
+    sources = [wk_hbm, wv_hbm, wq_hbm, winner_hbm, wsignal_hbm, wouter_hbm, wg_hbm]
     weight_copies = [
         pltpu.make_async_copy(ref, w_vmem.at[i], w_sem.at[i]) for i, ref in enumerate(sources)
     ]
@@ -379,10 +389,14 @@
         raw = jnp.dot(normed[...], w_vmem[index], preferred_element_type=jnp.float32)
         return (raw * scale).astype(jnp.bfloat16)
 
-    def nearest_first(i):
-        rising = jnp.where(i < plane, plane - 1 - i, i + 1)
-        falling = jnp.where(i < heads - 1 - plane, plane + 1 + i, heads - 2 - i)
-        return jnp.where(low, falling, rising)
+    half_planes = heads // 2
+    own_base = jnp.where(low, 0, half_planes)
+    far_base = half_planes - own_base
+
+    def order(k):
+        if k < half_planes:
+            return own_base + lax.rem(plane - own_base + k, half_planes)
+        return far_base + lax.rem(mirror - far_base + k - half_planes, half_planes)
 
     def q_copy(j):
         return remote(q_send.at[j], q_all.at[plane], q_s.at[j], q_r.at[plane], worker(j))
@@ -390,38 +404,39 @@
     def kv_copy(j):
         return remote(kv_send.at[j], kv_all.at[s], stage_s.at[j], stage_r.at[plane], worker(j))
 
-    def send_all(copy_of):
+    spare = heads + plane - own_base
+    spare_block = spare * RELAY + place
+
+    def near(k):
+        return heads + order(k) - own_base
+
+    def kv_mirror(i):
+        peer = order(i)
+        return remote(
+            kv_send.at[heads - 1 - peer],
+            kv_all.at[spare_block],
+            stage_s.at[near(i)],
+            stage_r.at[spare],
+            worker(peer),
+        )
+
+    def q_mirror(i):
+        peer = order(i)
+        return remote(
+            q_send.at[heads - 1 - peer],
+            q_all.at[spare],
+            q_s.at[near(i)],
+            q_r.at[spare],
+            worker(peer),
+        )
+
+    def away_only(action):
         @pl.when(t != y)
         def _():
-            copy_of(plane).start()
-
-        for i in range(heads - 1):
-            copy_of(nearest_first(i)).start()
-
-    def drain_all(copy_of):
-        for i in range(heads - 1):
-            copy_of(nearest_first(i)).wait_send()
-
-        @pl.when(t != y)
-        def _():
-            copy_of(plane).wait_send()
-
-    exponent = (lanes // 2) ** (-0.5) * math.log2(math.e)
-    projected = project(0, scale * exponent)
-    for h in range(heads):
-        q_send[h] = projected[:, h * lanes : (h + 1) * lanes]
-
-    @pl.when(home)
-    def _():
-        q_all[plane] = q_send[plane]
-
-    @pl.when(plane >= heads // 2)
-    def _():
-        meet()
-        send_all(q_copy)
+            action()
 
     for index in range(2):
-        projected = project(1 + index)
+        projected = project(index)
         for h in range(heads):
             kv_send[h, :, index * lanes : (index + 1) * lanes] = projected[
                 :, h * lanes : (h + 1) * lanes
@@ -431,54 +446,86 @@
     def _():
         kv_all[s] = kv_send[plane]
 
-    @pl.when(low)
-    def _():
-        meet()
-
-    send_all(kv_copy)
-
-    @pl.when(low)
-    def _():
-        send_all(q_copy)
-
-    def order(k):
-        return jnp.where(k <= plane, plane - k, k)
-
-    def block(plane_index, which):
-        return kv_all.at[plane_index * RELAY + which]
+    @pl.when(home)
+    def _():
+        kv_all[spare_block] = kv_send[mirror]
+
+    meet()
+
+    def block(slot, which):
+        return kv_all.at[slot * RELAY + which]
 
     def arrived(dst, recv_sem):
         remote(dst, dst, stage_s.at[0], recv_sem, x_dev).wait_recv()
 
-    def along_x(k):
-        here = block(order(k), member)
-        return remote(here, here, x_s.at[k], x_r.at[order(k)], x_dev)
-
-    def across(k):
-        here = block(order(k), member)
-        return remote(here, here, c_s.at[k], c_r.at[order(k)], c_dev)
-
-    def onward(k):
-        from_x = block(order(k), member + 1 - 2 * x)
-        return remote(from_x, from_x, d_s.at[k], d_r.at[order(k)], c_dev)
-
-    def forward_stage(k):
-        along_x(k).start()
-        across(k).start()
-
-    def forward_square(k):
-        c = order(k)
-        arrived(block(c, member + 1 - 2 * x), x_r.at[c])
-        onward(k).start()
-
-    def finish_plane(k):
-        c = order(k)
-        arrived(block(c, lax.rem(member + 2, RELAY)), c_r.at[c])
-        arrived(block(c, RELAY - 1 - member), d_r.at[c])
+    def along_x(slot):
+        here = block(slot, member)
+        return remote(here, here, x_s.at[slot], x_r.at[slot], x_dev)
+
+    def across(slot):
+        here = block(slot, member)
+        return remote(here, here, c_s.at[slot], c_r.at[slot], c_dev)
+
+    def onward(slot):
+        from_x = block(slot, member + 1 - 2 * x)
+        return remote(from_x, from_x, d_s.at[slot], d_r.at[slot], c_dev)
+
+    def forward_stage(slot):
+        along_x(slot).start()
+        across(slot).start()
+
+    def receive(slot):
+        arrived(block(slot, member), stage_r.at[slot])
+        forward_stage(slot)
+
+    def forward_square(slot):
+        arrived(block(slot, member + 1 - 2 * x), x_r.at[slot])
+        onward(slot).start()
+
+    def finish_plane(slot):
+        arrived(block(slot, lax.rem(member + 2, RELAY)), c_r.at[slot])
+        arrived(block(slot, RELAY - 1 - member), d_r.at[slot])
+
+    def first_sends():
+        for k in range(1, half_planes):
+            kv_copy(order(k)).start()
+
+        @pl.when(low)
+        def _():
+            kv_copy(mirror).start()
 
     @pl.when(home)
     def _():
-        forward_stage(0)
+        forward_stage(plane)
+        first_sends()
+
+    away_only(lambda: kv_copy(plane).start())
+
+    exponent = (lanes // 2) ** (-0.5) * math.log2(math.e)
+    projected = project(2, scale * exponent)
+    for h in range(heads):
+        q_send[h] = projected[:, h * lanes : (h + 1) * lanes]
+
+    @pl.when(home)
+    def _():
+        q_all[plane] = q_send[plane]
+
+    @pl.when(home)
+    def _():
+        q_all[spare] = q_send[mirror]
+
+    @pl.when(t != y)
+    def _():
+        q_copy(plane).start()
+        first_sends()
+
+    for k in range(1, half_planes):
+        q_copy(order(k)).start()
+
+    @pl.when(high)
+    def _():
+        for k in range(half_planes, heads):
+            q_copy(order(k)).start()
 
     inner = project(3).astype(jnp.float32)
     signal_f = project(4).astype(jnp.float32)
@@ -496,16 +543,30 @@
     def _():
         tail_copy.start()
 
+    @pl.when(low)
+    def _():
+        for k in range(half_planes + 1, heads):
+            kv_copy(order(k)).start()
+
+    @pl.when(home)
+    def _():
+        forward_stage(spare)
+
     @pl.when(t != y)
     def _():
-        arrived(block(plane, member), stage_r.at[plane])
-        forward_stage(0)
-
+        kv_mirror(0).start()
+        q_mirror(0).start()
+
+    for i in range(1, half_planes):
+        kv_mirror(i).start()
+        q_mirror(i).start()
+
+    away_only(lambda: receive(plane))
     small[4].wait()
     outer[...] = project(5)
     gate = project(6).astype(jnp.float32)
     opened[...] = gate / (1.0 + jnp.exp(-gate)) * head_gain_ref[...]
-    forward_square(0)
+    forward_square(plane)
 
     span = RELAY * rows
     lane = lax.broadcasted_iota(jnp.int32, (1, lanes), 1)
@@ -514,27 +575,26 @@
         for of_map in (lane < lanes // 2, lane >= lanes // 2)
     ]
 
-    def attend_plane(c):
-        held = kv_all[c * RELAY : (c + 1) * RELAY].reshape(span, 2 * lanes)
-        keys = held[:, :lanes]
-        values = jnp.concatenate(
-            [held[:, lanes:], jnp.ones((span, lanes), jnp.bfloat16)], axis=1
-        )
-
-        def scores(qi, m):
+    def attend(tiles):
+        def scores(qi, c, diagonal, m):
+            keys = kv_all[pl.ds(c * RELAY, RELAY)].reshape(span, 2 * lanes)[:, :lanes]
             score = lax.dot_general(
                 q_all[qi] * masks[m],
                 keys,
                 (((1,), (1,)), ((), ())),
                 preferred_element_type=jnp.float32,
             )
-            if qi == c:
+            if diagonal:
                 row = lax.broadcasted_iota(jnp.int32, (rows, span), 0) + member * rows
                 col = lax.broadcasted_iota(jnp.int32, (rows, span), 1)
                 score = jnp.where(row >= col, score, -1e30)
             return score
 
-        def absorb(at_row, score):
+        def absorb(at_row, c, score):
+            held = kv_all[pl.ds(c * RELAY, RELAY)].reshape(span, 2 * lanes)
+            values = jnp.concatenate(
+                [held[:, lanes:], jnp.ones((span, lanes), jnp.bfloat16)], axis=1
+            )
             before = row_max[at_row]
             top = jnp.maximum(before, jnp.max(score, axis=-1, keepdims=True))
             weights = jnp.exp2(score - top[:, :1]).astype(jnp.bfloat16)
@@ -544,55 +604,113 @@
             for part in (slice(0, lanes), slice(lanes, 2 * lanes)):
                 accum[at_row, :, part] = accum[at_row, :, part] * factor + update[:, part]
 
-        items = [(qi, m) for qi in range(heads - 1, c - 1, -1) for m in range(2)]
+        items = [(*tile, m) for tile in tiles for m in range(2)]
         upcoming = scores(*items[0])
-        for i, (qi, m) in enumerate(items):
+        for i, (qi, c, _, m) in enumerate(items):
             score = upcoming
             if i + 1 < len(items):
                 upcoming = scores(*items[i + 1])
-            absorb(2 * qi + m, score)
-
-    lam_pick = lax.broadcasted_iota(jnp.int32, (1, heads), 1) == plane
+            absorb(2 * qi + m, c, score)
+
+    def attend_triangle(base):
+        below = [
+            (base + i, base + j, False)
+            for j in range(half_planes)
+            for i in range(j + 1, half_planes)
+        ]
+        attend(below + [(base + i, base + i, True) for i in range(half_planes)])
+
+    def attend_row(q):
+        attend([(q, j, False) for j in range(half_planes)])
+
+    lam_index = lax.broadcasted_iota(jnp.int32, (1, heads), 1)
     lam_out.wait()
     lam_row = jnp.where(home, lam_own[...], lam_other[...])
-    lam = jnp.sum(jnp.where(lam_pick, lam_row, 0.0), axis=-1, keepdims=True)
+
+    def lambda_of(head):
+        return jnp.sum(jnp.where(lam_index == head, lam_row, 0.0), axis=-1, keepdims=True)
+
     column = lax.broadcasted_iota(jnp.int32, (rows, lanes), 1)
 
-    def o_copy(q):
-        return remote(o_send.at[q], o_all.at[plane], o_s.at[q], o_r.at[plane], worker(q))
-
-    def lt_copy(q):
-        return remote(lt_send.at[q], lt_all.at[plane], lt_s.at[q], lt_r.at[plane], worker(q))
-
-    def finalize(q):
+    def slot_of(q, mirrored):
+        return heads + q - own_base if mirrored else q
+
+    def o_copies(q, mirrored):
+        slot = slot_of(q, mirrored)
+        head = mirror if mirrored else plane
+        return [
+            remote(o_send.at[slot], o_all.at[head], o_s.at[slot], o_r.at[head], worker(q)),
+            remote(lt_send.at[slot], lt_all.at[head], lt_s.at[slot], lt_r.at[head], worker(q)),
+        ]
+
+    def p_copies(q, mirrored):
+        at_row = q - half_planes
+        to = half_planes + mirror if mirrored else plane
+        return [
+            remote(p_send.at[at_row], p_all.at[to], p_s.at[at_row], p_r.at[to], worker(q)),
+            remote(pl_send.at[at_row], pl_all.at[to], pl_s.at[at_row], pl_r.at[to], worker(q)),
+        ]
+
+    def settle(q, copies, pairs):
+        away = (q != plane) | (t != y)
+
+        @pl.when(away)
+        def _():
+            for copy in copies:
+                copy.start()
+
+        @pl.when(jnp.logical_not(away))
+        def _():
+            for into, index, value in pairs:
+                into[index] = value[...]
+
+    def partial(q, mirrored):
+        slot = slot_of(q, mirrored)
+        at_row = q - half_planes
+        logs = []
+        for m in range(2):
+            held = accum[2 * slot + m]
+            total = held[:, lanes:]
+            p_send[at_row, m * rows : (m + 1) * rows, :] = (held[:, :lanes] / total).astype(
+                jnp.bfloat16
+            )
+            logs.append(jnp.log(total) + row_max[2 * slot + m] * math.log(2.0))
+        turned = jnp.where(column == 0, logs[0], logs[1]).T
+        pl_send[at_row] = turned[:2, :]
+        if mirrored:
+            to = half_planes + mirror
+            settle(
+                q,
+                p_copies(q, mirrored),
+                [(p_all, to, p_send.at[at_row]), (pl_all, to, pl_send.at[at_row])],
+            )
+        else:
+            for copy in p_copies(q, mirrored):
+                copy.start()
+
+    def finalize(q, mirrored):
+        slot = slot_of(q, mirrored)
+        head = mirror if mirrored else plane
         maps = []
         logs = []
         for m in range(2):
-            held = accum[2 * q + m]
+            held = accum[2 * slot + m]
             total = held[:, lanes:]
             maps.append(held[:, :lanes] / total)
-            logs.append(jnp.log(total) + row_max[2 * q + m] * math.log(2.0))
-        diff = maps[0] - lam * maps[1]
+            logs.append(jnp.log(total) + row_max[2 * slot + m] * math.log(2.0))
+        diff = maps[0] - lambda_of(head) * maps[1]
         mean = jnp.mean(diff * diff, axis=-1, keepdims=True)
-        o_send[q] = (diff * lax.rsqrt(mean + 1e-05)).astype(jnp.bfloat16)
+        o_send[slot] = (diff * lax.rsqrt(mean + 1e-05)).astype(jnp.bfloat16)
         turned = jnp.where(column == 0, logs[0], logs[1]).T
-        lt_send[q] = turned[:2, :]
-        away = (q != plane) | (t != y)
-
-        @pl.when(away)
-        def _():
-            o_copy(q).start()
-            lt_copy(q).start()
-
-        @pl.when(jnp.logical_not(away))
-        def _():
-            o_all[plane] = o_send[q]
-            lt_all[plane] = lt_send[q]
-
-    def q_arrived(q):
-        @pl.when((q != plane) | (t != y))
-        def _():
-            arrived(q_all.at[q], q_r.at[q])
+        lt_send[slot] = turned[:2, :]
+        settle(
+            q,
+            o_copies(q, mirrored),
+            [(o_all, head, o_send.at[slot]), (lt_all, head, lt_send.at[slot])],
+        )
+
+    def q_arrived(slot):
+        arrived(q_all.at[slot], q_r.at[slot])
 
     def convolve():
         small[3].wait()
@@ -621,56 +739,141 @@
             conv_out[...], wc_vmem[...], preferred_element_type=jnp.float32
         )
 
-    @pl.loop(0, heads)
-    def _(k):
-        c = order(k)
-
-        @pl.when(k + 1 < heads)
-        def _():
-            following = order(k + 1)
-            arrived(block(following, member), stage_r.at[following])
-            forward_stage(k + 1)
-
-        @pl.loop(c, heads)
+    def far_slots():
+        return [order(k) for k in range(half_planes, heads)]
+
+    for k in range(1, half_planes):
+        receive(order(k))
+    for k in range(1, half_planes):
+        forward_square(order(k))
+    for k in range(half_planes):
+        finish_plane(order(k))
+
+    @pl.when(low)
+    def _():
+        for slot in far_slots():
+            q_arrived(slot)
+
+        @pl.loop(half_planes, heads)
         def _(q):
-            @pl.when((k == 0) | ((q == c) & (k <= plane)))
-            def _():
-                q_arrived(q)
-
-        finish_plane(k)
-        for cc in range(heads):
-
-            @pl.when(c == cc)
-            def _(cc=cc):
-                attend_plane(cc)
-
-        @pl.when(k + 1 < heads)
-        def _():
-            forward_square(k + 1)
-
-        @pl.loop(0, heads)
+            attend_row(q)
+            partial(q, False)
+
+    away_only(lambda: q_arrived(plane))
+    for k in range(1, half_planes):
+        q_arrived(order(k))
+    attend_triangle(own_base)
+
+    @pl.when(low)
+    def _():
+        @pl.loop(0, half_planes)
         def _(q):
-            @pl.when(((k == plane) & (q <= plane)) | ((k > plane) & (q == c)))
-            def _():
-                finalize(q)
-
-        @pl.when(k == 0)
-        def _():
-            convolve()
+            finalize(q, False)
+
+    away_only(lambda: receive(spare))
+    for k in range(1, half_planes):
+        receive(near(k))
+
+    @pl.when(high)
+    def _():
+        for slot in far_slots():
+            receive(slot)
+
+    convolve()
+    for k in range(half_planes):
+        forward_square(near(k))
+    for k in range(half_planes):
+        finish_plane(near(k))
+        if k == 0:
+            away_only(lambda: q_arrived(spare))
+        else:
+            q_arrived(near(k))
+    attend_triangle(heads)
+
+    @pl.when(low)
+    def _():
+        @pl.loop(0, half_planes)
+        def _(q):
+            finalize(q, True)
+
+    @pl.when(high)
+    def _():
+        for slot in far_slots():
+            forward_square(slot)
+
+        @pl.loop(half_planes, heads)
+        def _(q):
+            partial(q, True)
+
+        for slot in far_slots():
+            finish_plane(slot)
+
+        @pl.loop(half_planes, heads)
+        def _(q):
+            attend_row(q)
+            finalize(q, False)
 
     weight_copies[len(sources) + 1].wait()
     half_rows = rows // 2
+
+    def from_elsewhere(j):
+        return (t != y) | ((j != plane) & (j != mirror))
+
     for j in range(heads):
 
-        @pl.when((j != plane) | (t != y))
+        @pl.when(from_elsewhere(j) if j >= half_planes else (low & ((t != y) | (j != plane))))
         def _(j=j):
             arrived(o_all.at[j], o_r.at[j])
             arrived(lt_all.at[j], lt_r.at[j])
 
-    for h in range(heads):
+    def whole(h):
         totals_ref[h] = lt_all[h]
         part = slice(h * lanes, (h + 1) * lanes)
         head_out[:, part] = (o_all[h].astype(jnp.float32) * opened[:, part]).astype(jnp.bfloat16)
+
+    def merged(h):
+        arrived(p_all.at[h], p_r.at[h])
+        arrived(pl_all.at[h], pl_r.at[h])
+        second = half_planes + h
+
+        @pl.when((t != y) | (h != mirror))
+        def _():
+            arrived(p_all.at[second], p_r.at[second])
+            arrived(pl_all.at[second], pl_r.at[second])
+
+        top = jnp.maximum(pl_all[h], pl_all[second])
+        shares = [jnp.exp(pl_all[h] - top), jnp.exp(pl_all[second] - top)]
+        total = shares[0] + shares[1]
+        totals_ref[h] = top + jnp.log(total)
+        turned = jnp.concatenate(
+            [shares[0] / total, shares[1] / total, jnp.zeros((4, rows), jnp.float32)], axis=0
+        ).T
+        maps = []
+        for m in range(2):
+            held = slice(m * rows, (m + 1) * rows)
+            maps.append(
+                turned[:, m : m + 1] * p_all[h, held, :].astype(jnp.float32)
+                + turned[:, 2 + m : 3 + m] * p_all[second, held, :].astype(jnp.float32)
+            )
+        diff = maps[0] - lam_own[:, h : h + 1] * maps[1]
+        mean = jnp.mean(diff * diff, axis=-1, keepdims=True)
+        part = slice(h * lanes, (h + 1) * lanes)
+        head_out[:, part] = (diff * lax.rsqrt(mean + 1e-05) * opened[:, part]).astype(
+            jnp.bfloat16
+        )
+
+    for h in range(half_planes, heads):
+        whole(h)
+
+    @pl.when(low)
+    def _():
+        for h in range(half_planes):
+            whole(h)
+
+    @pl.when(high)
+    def _():
+        for h in range(half_planes):
+            merged(h)
 
     def partial_rows(which):
         there = pl.ds(pl.multiple_of(which * half_rows, half_rows), half_rows)
@@ -683,14 +886,50 @@
     own_rows = partial_rows(t).astype(jnp.float32)
     exchange.wait()
     mixed_ref[...] = (own_rows + part_recv[...].astype(jnp.float32)).astype(jnp.bfloat16)
-    for k in range(heads):
-        along_x(k).wait_send()
-        across(k).wait_send()
-        onward(k).wait_send()
-    drain_all(q_copy)
-    drain_all(kv_copy)
-    drain_all(o_copy)
-    drain_all(lt_copy)
+    def drain(slot):
+        along_x(slot).wait_send()
+        across(slot).wait_send()
+        onward(slot).wait_send()
+
+    def drain_o(q, copies):
+        @pl.when((q != plane) | (t != y))
+        def _():
+            for copy in copies:
+                copy.wait_send()
+
+    for k in range(half_planes):
+
+        def sent(k=k):
+            kv_copy(order(k)).wait_send()
+            q_copy(order(k)).wait_send()
+            kv_mirror(k).wait_send()
+            q_mirror(k).wait_send()
+
+        if k == 0:
+            away_only(sent)
+        else:
+            sent()
+        drain(order(k))
+        drain(near(k))
+
+    @pl.when(low)
+    def _():
+        for slot in far_slots():
+            kv_copy(slot).wait_send()
+        for q in range(half_planes):
+            drain_o(q, o_copies(q, False))
+            drain_o(q, o_copies(q, True))
+            for copy in p_copies(half_planes + q, False):
+                copy.wait_send()
+
+    @pl.when(high)
+    def _():
+        for slot in far_slots():
+            q_copy(slot).wait_send()
+            drain(slot)
+        for q in range(half_planes, heads):
+            drain_o(q, o_copies(q, False))
+            drain_o(q, p_copies(q, True))
 
     @pl.when(s < last)
     def _():
@@ -704,6 +943,7 @@
     heads = lambdas.shape[0]
     local = wq.shape[1]
     lanes = local // heads
+    slots = heads + heads // 2
     out_width = args[12].shape[1]
     bf16, f32 = jnp.bfloat16, jnp.float32
     vmem = pl.BlockSpec(memory_space=pltpu.VMEM)
@@ -735,10 +975,10 @@
             pltpu.VMEM(args[13].shape, bf16),
             pltpu.VMEM((heads, rows, 2 * lanes), bf16),
             pltpu.VMEM((heads, rows, lanes), bf16),
-            pltpu.VMEM((sp_count, rows, 2 * lanes), bf16),
-            pltpu.VMEM((heads, rows, lanes), bf16),
-            pltpu.VMEM((2 * heads, rows, lanes), f32),
-            pltpu.VMEM((2 * heads, rows, 2 * lanes), f32),
+            pltpu.VMEM((slots * RELAY, rows, 2 * lanes), bf16),
+            pltpu.VMEM((slots, rows, lanes), bf16),
+            pltpu.VMEM((2 * slots, rows, lanes), f32),
+            pltpu.VMEM((2 * slots, rows, 2 * lanes), f32),
             pltpu.VMEM((rows, local), f32),
             pltpu.VMEM((rows, local), bf16),
             pltpu.VMEM((rows, local), bf16),
@@ -747,9 +987,13 @@
             pltpu.VMEM((rows, local), bf16),
             pltpu.VMEM((rows, local), bf16),
             pltpu.VMEM((rows, out_width), f32),
+            pltpu.VMEM((slots, rows, lanes), bf16),
             pltpu.VMEM((heads, rows, lanes), bf16),
-            pltpu.VMEM((heads, rows, lanes), bf16),
+            pltpu.VMEM((slots, 2, rows), f32),
             pltpu.VMEM((heads, 2, rows), f32),
+            pltpu.VMEM((heads // 2, 2 * rows, lanes), bf16),
+            pltpu.VMEM((heads, 2 * rows, lanes), bf16),
+            pltpu.VMEM((heads // 2, 2, rows), f32),
             pltpu.VMEM((heads, 2, rows), f32),
             pltpu.VMEM((rows // 2, out_width), bf16),
             pltpu.VMEM((rows // 2, out_width), bf16),
@@ -759,7 +1003,7 @@
             dma((2,)),
             dma((2,)),
         ]
-        + [dma((heads,)) for _ in range(14)]
+        + [dma((slots,)) for _ in range(18)]
         + [pltpu.SemaphoreType.REGULAR, pltpu.SemaphoreType.REGULAR],
         compiler_params=pltpu.CompilerParams(
             collective_id=0, has_side_effects=True, vmem_limit_bytes=60 * 1024 * 1024
@@ -772,6 +1016,7 @@
         mesh.shape["tp"] == 2
         and mesh.shape["sp"] == heads * RELAY
         and heads > 1
+        and heads % 2 == 0
         and rows % 32 == 0
         and key_columns == value_columns == heads * 128
     )

time: 52.5 us -> 50.2 us (0.956)
  the two profiles are of different devices: /device:TPU:0 before, /device:TPU:17 now
where the time goes in v3:
time: 50.2 us; the launch traced here: 49.6 us
  Pallas kernels  45.8 us (91%)
  local copies, waits for them, and re-layouts  3.18 us (6%)
  between operations  0.64 us (1%)
    pallas_call x1, Pallas kernels, fused(): pl.pallas_call(functools.partial(fused_kernel, sp_count, heads), out_shap...  45.8 us
    unnamed x2, local copies, waits for them, and re-layouts  3.18 us

profile of v3, /device:TPU:17, one launch (start us, length us, event | category | flops | bytes accessed | tf_op | source)
XLA Modules:
  0.0 49.6 jit_solution(11635081542284233208)
XLA Ops:
  0.6 45.8 %shard_map.149 = (bf16[128,2048]{1,0:T(8,128)(2,1)}, f32[4,2,256]{2,1,0:T(2,128)}) custom-call(bf16[256,1024]{1,0:T(8,128)(2,1)} %tokens_hbm.1, f32[1,2048]{1,0:T(1,128)} %bitcast.3, bf16[2048,512]{1,0:T(8,128)(2,1)} %wq_hbm.1, bf16[2048,512]{1,0:T(8,128)(2,1)} %wk_hbm.1, bf16[2048,512]{1,0:T(8,128)(2,1)} %wv_hbm.1, bf16[2048,512]{1,0:T(8,128)(2,1)} %wg_hbm.1, ...), custom_call_target="tpu_custom_call" | custom-call | tf_op jit(solution)/shard_map/pallas_call | solution.py:956
  46.4 1.9 %copy.18 = bf16[128,2048]{1,0:T(8,128)(2,1)} copy(bf16[128,2048]{1,0:T(8,128)(2,1)} %get-tuple-element.4) | data formatting | bytes 1048576
  48.3 1.3 %copy.19 = f32[4,2,256]{2,1,0:T(2,128)} copy(f32[4,2,256]{2,1,0:T(2,128)} %get-tuple-element.5) | data formatting | bytes 16384

commit v4 on v3

--- a/solution.py
+++ b/solution.py
@@ -167,6 +167,7 @@
 
 
 RELAY = 4
+PIECES = 4
 
 
 def fused_kernel(
@@ -543,30 +544,49 @@
     def _():
         tail_copy.start()
 
-    @pl.when(low)
-    def _():
-        for k in range(half_planes + 1, heads):
-            kv_copy(order(k)).start()
-
-    @pl.when(home)
-    def _():
-        forward_stage(spare)
-
-    @pl.when(t != y)
-    def _():
-        kv_mirror(0).start()
-        q_mirror(0).start()
-
-    for i in range(1, half_planes):
-        kv_mirror(i).start()
-        q_mirror(i).start()
-
-    away_only(lambda: receive(plane))
     small[4].wait()
     outer[...] = project(5)
     gate = project(6).astype(jnp.float32)
     opened[...] = gate / (1.0 + jnp.exp(-gate)) * head_gain_ref[...]
+    @pl.when(low)
+    def _():
+        for k in range(half_planes + 1, heads):
+            kv_copy(order(k)).start()
+
+    @pl.when(home)
+    def _():
+        forward_stage(spare)
+
+    @pl.when(t != y)
+    def _():
+        kv_mirror(0).start()
+        q_mirror(0).start()
+
+    for i in range(1, half_planes):
+        kv_mirror(i).start()
+        q_mirror(i).start()
+
+    away_only(lambda: receive(plane))
+    for k in range(1, half_planes):
+        receive(order(k))
     forward_square(plane)
+    away_only(lambda: receive(spare))
+
+    @pl.when(high)
+    def _():
+        receive(mirror)
+
+    for k in range(1, half_planes):
+        forward_square(order(k))
+    for k in range(1, half_planes):
+        receive(near(k))
+
+    @pl.when(high)
+    def _():
+        for k in range(half_planes + 1, heads):
+            receive(order(k))
+
+    forward_square(spare)
 
     span = RELAY * rows
     lane = lax.broadcasted_iota(jnp.int32, (1, lanes), 1)
@@ -742,10 +762,6 @@
     def far_slots():
         return [order(k) for k in range(half_planes, heads)]
 
-    for k in range(1, half_planes):
-        receive(order(k))
-    for k in range(1, half_planes):
-        forward_square(order(k))
     for k in range(half_planes):
         finish_plane(order(k))
 
@@ -770,17 +786,8 @@
         def _(q):
             finalize(q, False)
 
-    away_only(lambda: receive(spare))
+    convolve()
     for k in range(1, half_planes):
-        receive(near(k))
-
-    @pl.when(high)
-    def _():
-        for slot in far_slots():
-            receive(slot)
-
-    convolve()
-    for k in range(half_planes):
         forward_square(near(k))
     for k in range(half_planes):
         finish_plane(near(k))
@@ -808,21 +815,18 @@
         for slot in far_slots():
             finish_plane(slot)
 
+        attend([(half_planes + i, j, False) for j in range(half_planes) for i in range(half_planes)])
+
         @pl.loop(half_planes, heads)
         def _(q):
-            attend_row(q)
             finalize(q, False)
 
     weight_copies[len(sources) + 1].wait()
     half_rows = rows // 2
 
-    def from_elsewhere(j):
-        return (t != y) | ((j != plane) & (j != mirror))
-
-    for j in range(heads):
-
-        @pl.when(from_elsewhere(j) if j >= half_planes else (low & ((t != y) | (j != plane))))
-        def _(j=j):
+    def from_worker(j, here):
+        @pl.when((t != y) | (plane != here))
+        def _():
             arrived(o_all.at[j], o_r.at[j])
             arrived(lt_all.at[j], lt_r.at[j])
 
@@ -862,12 +866,12 @@
             jnp.bfloat16
         )
 
-    for h in range(half_planes, heads):
-        whole(h)
+    split = half_planes * lanes
 
     @pl.when(low)
     def _():
         for h in range(half_planes):
+            from_worker(h, h)
             whole(h)
 
     @pl.when(high)
@@ -875,17 +879,45 @@
         for h in range(half_planes):
             merged(h)
 
-    def partial_rows(which):
+    conv_part[...] += jnp.dot(
+        head_out[:, :split], wo_vmem[:split, :], preferred_element_type=jnp.float32
+    )
+    for h in range(half_planes, heads):
+
+        @pl.when(low)
+        def _(h=h):
+            from_worker(h, heads - 1 - h)
+
+        @pl.when(high)
+        def _(h=h):
+            from_worker(h, h)
+
+        whole(h)
+
+    pieces, _, breadth = part_send.shape
+
+    def partial_rows(which, piece):
         there = pl.ds(pl.multiple_of(which * half_rows, half_rows), half_rows)
-        attn = jnp.dot(head_out[there, :], wo_vmem[...], preferred_element_type=jnp.float32)
-        return (attn + conv_part[there, :]).astype(jnp.bfloat16)
-
-    part_send[...] = partial_rows(1 - t)
-    exchange = remote(part_send, part_recv, part_sem.at[0], part_sem.at[1], c_dev)
-    exchange.start()
-    own_rows = partial_rows(t).astype(jnp.float32)
-    exchange.wait()
-    mixed_ref[...] = (own_rows + part_recv[...].astype(jnp.float32)).astype(jnp.bfloat16)
+        columns = slice(piece * breadth, (piece + 1) * breadth)
+        attn = jnp.dot(
+            head_out[there, split:], wo_vmem[split:, columns], preferred_element_type=jnp.float32
+        )
+        return (attn + conv_part[there, columns]).astype(jnp.bfloat16)
+
+    exchanges = [
+        remote(part_send.at[i], part_recv.at[i], part_sem.at[i], part_sem.at[pieces + i], c_dev)
+        for i in range(pieces)
+    ]
+    for i in range(pieces):
+        part_send[i] = partial_rows(1 - t, i)
+        exchanges[i].start()
+    for i in range(pieces):
+        own_rows = partial_rows(t, i).astype(jnp.float32)
+        exchanges[i].wait()
+        mixed_ref[:, i * breadth : (i + 1) * breadth] = (
+            own_rows + part_recv[i].astype(jnp.float32)
+        ).astype(jnp.bfloat16)
+
     def drain(slot):
         along_x(slot).wait_send()
         across(slot).wait_send()
@@ -995,13 +1027,13 @@
             pltpu.VMEM((heads, 2 * rows, lanes), bf16),
             pltpu.VMEM((heads // 2, 2, rows), f32),
             pltpu.VMEM((heads, 2, rows), f32),
-            pltpu.VMEM((rows // 2, out_width), bf16),
-            pltpu.VMEM((rows // 2, out_width), bf16),
+            pltpu.VMEM((PIECES, rows // 2, out_width // PIECES), bf16),
+            pltpu.VMEM((PIECES, rows // 2, out_width // PIECES), bf16),
             dma((9,)),
             dma((5,)),
             dma((4,)),
             dma((2,)),
-            dma((2,)),
+            dma((2 * PIECES,)),
         ]
         + [dma((slots,)) for _ in range(18)]
         + [pltpu.SemaphoreType.REGULAR, pltpu.SemaphoreType.REGULAR],

time: 50.2 us -> 45.7 us (0.910)
  Pallas kernels: 45.8 us -> 41.7 us
    pallas_call x1, Pallas kernels: 45.8 us -> 41.7 us  [fused(): pl.pallas_call(functools.partial(fused_kernel, sp_count, heads), out_shap...]
where the time goes in v4:
time: 45.7 us; the launch traced here: 45.5 us
  Pallas kernels  41.7 us (91%)
  local copies, waits for them, and re-layouts  3.18 us (7%)
  between operations  0.64 us (1%)
    pallas_call x1, Pallas kernels, fused(): pl.pallas_call(functools.partial(fused_kernel, sp_count, heads), out_shap...  41.7 us
    unnamed x2, local copies, waits for them, and re-layouts  3.18 us

profile of v4, /device:TPU:17, one launch (start us, length us, event | category | flops | bytes accessed | tf_op | source)
XLA Modules:
  0.0 45.5 jit_solution(13561291721194058900)
XLA Ops:
  0.6 41.7 %shard_map.149 = (bf16[128,2048]{1,0:T(8,128)(2,1)}, f32[4,2,256]{2,1,0:T(2,128)}) custom-call(bf16[256,1024]{1,0:T(8,128)(2,1)} %tokens_hbm.1, f32[1,2048]{1,0:T(1,128)} %bitcast.3, bf16[2048,512]{1,0:T(8,128)(2,1)} %wq_hbm.1, bf16[2048,512]{1,0:T(8,128)(2,1)} %wk_hbm.1, bf16[2048,512]{1,0:T(8,128)(2,1)} %wv_hbm.1, bf16[2048,512]{1,0:T(8,128)(2,1)} %wg_hbm.1, ...), custom_call_target="tpu_custom_call" | custom-call | tf_op jit(solution)/shard_map/pallas_call | solution.py:988
  42.3 1.9 %copy.18 = bf16[128,2048]{1,0:T(8,128)(2,1)} copy(bf16[128,2048]{1,0:T(8,128)(2,1)} %get-tuple-element.4) | data formatting | bytes 1048576
  44.2 1.3 %copy.19 = f32[4,2,256]{2,1,0:T(2,128)} copy(f32[4,2,256]{2,1,0:T(2,128)} %get-tuple-element.5) | data formatting | bytes 16384

commit v5 on v4

--- a/solution.py
+++ b/solution.py
@@ -988,8 +988,8 @@
     return pl.pallas_call(
         functools.partial(fused_kernel, sp_count, heads),
         out_shape=(
-            jax.ShapeDtypeStruct((rows // 2, out_width), bf16),
-            jax.ShapeDtypeStruct((heads, 2, rows), f32),
+            pltpu.VMEM((rows // 2, out_width), bf16),
+            pltpu.VMEM((heads, 2, rows), f32),
         ),
         in_specs=[hbm] * len(operands),
         out_specs=(vmem, vmem),
@@ -1038,7 +1038,7 @@
         + [dma((slots,)) for _ in range(18)]
         + [pltpu.SemaphoreType.REGULAR, pltpu.SemaphoreType.REGULAR],
         compiler_params=pltpu.CompilerParams(
-            collective_id=0, has_side_effects=True, vmem_limit_bytes=60 * 1024 * 1024
+            collective_id=0, has_side_effects=True, vmem_limit_bytes=(60 * 1024 - 4000) * 1024
         ),
     )(*operands)
 

time: 45.7 us -> 43.1 us (0.943)
  local copies, waits for them, and re-layouts: 3.18 us -> 1.39 us
  Pallas kernels: 41.7 us -> 40.9 us
    unnamed x2, local copies, waits for them, and re-layouts: 3.18 us -> 1.39 us
    pallas_call x1, Pallas kernels: 41.7 us -> 40.9 us  [fused(): pl.pallas_call(functools.partial(fused_kernel, sp_count, heads), out_shap...]
where the time goes in v5:
time: 43.1 us; the launch traced here: 43 us
  Pallas kernels  40.9 us (95%)
  local copies, waits for them, and re-layouts  1.39 us (3%)
  between operations  0.64 us (1%)
    pallas_call x1, Pallas kernels, fused(): pl.pallas_call(functools.partial(fused_kernel, sp_count, heads), out_shap...  40.9 us
    unnamed x2, local copies, waits for them, and re-layouts  1.39 us

profile of v5, /device:TPU:17, one launch (start us, length us, event | category | flops | bytes accessed | tf_op | source)
XLA Modules:
  0.0 43.0 jit_solution(10658605272213915380)
XLA Ops:
  0.6 40.9 %shard_map.149 = (bf16[128,2048]{1,0:T(8,128)(2,1)S(1)}, f32[4,2,256]{2,1,0:T(2,128)S(1)}) custom-call(bf16[256,1024]{1,0:T(8,128)(2,1)} %tokens_hbm.1, f32[1,2048]{1,0:T(1,128)} %bitcast.3, bf16[2048,512]{1,0:T(8,128)(2,1)} %wq_hbm.1, bf16[2048,512]{1,0:T(8,128)(2,1)} %wk_hbm.1, bf16[2048,512]{1,0:T(8,128)(2,1)} %wv_hbm.1, bf16[2048,512]{1,0:T(8,128)(2,1)} %wg_hbm.1, ...), custom_call_target="tpu_custom_call" | custom-call | tf_op jit(solution)/shard_map/pallas_call | solution.py:988
  41.6 0.8 %copy.18 = bf16[128,2048]{1,0:T(8,128)(2,1)} copy(bf16[128,2048]{1,0:T(8,128)(2,1)S(1)} %get-tuple-element.2) | data formatting | bytes 1048576
  42.4 0.6 %copy.19 = f32[4,2,256]{2,1,0:T(2,128)} copy(f32[4,2,256]{2,1,0:T(2,128)S(1)} %get-tuple-element.3) | data formatting | bytes 16384

commit v6 on v5

--- a/solution.py
+++ b/solution.py
@@ -364,7 +364,7 @@
     small[0].wait()
     tokens_out = remote(own_tokens, other_tokens, tok_sem.at[0], tok_sem.at[1], c_dev)
     tokens_out.start()
-    for copy in weight_copies[1:]:
+    for copy in weight_copies[1:3]:
         copy.start()
     small[2].wait()
     lam_out = remote(lam_own, lam_other, tok_sem.at[2], tok_sem.at[3], c_dev)
@@ -378,16 +378,31 @@
     theirs = pl.ds(pl.multiple_of((1 - t) * half, half), half)
     own_f = own_tokens[...].astype(jnp.float32)
     squares = jnp.sum(own_f * own_f, axis=-1, keepdims=True)
-    normed[:, mine] = (own_f * gain_ref[:, mine]).astype(jnp.bfloat16)
+    own_normed = (own_f * gain_ref[:, mine]).astype(jnp.bfloat16)
+    normed[:, mine] = own_normed
+    early = []
+    for index in range(3):
+        weight_copies[index].wait()
+        early.append(
+            jnp.dot(own_normed, w_vmem[index, mine, :], preferred_element_type=jnp.float32)
+        )
+    for copy in weight_copies[3:]:
+        copy.start()
     tokens_out.wait()
     other_f = other_tokens[...].astype(jnp.float32)
     squares = squares + jnp.sum(other_f * other_f, axis=-1, keepdims=True)
-    normed[:, theirs] = (other_f * gain_ref[:, theirs]).astype(jnp.bfloat16)
+    other_normed = (other_f * gain_ref[:, theirs]).astype(jnp.bfloat16)
+    normed[:, theirs] = other_normed
     scale = lax.rsqrt(squares / width + 1e-06)
 
     def project(index, scale=scale):
-        weight_copies[index].wait()
-        raw = jnp.dot(normed[...], w_vmem[index], preferred_element_type=jnp.float32)
+        if index < len(early):
+            raw = early[index] + jnp.dot(
+                other_normed, w_vmem[index, theirs, :], preferred_element_type=jnp.float32
+            )
+        else:
+            weight_copies[index].wait()
+            raw = jnp.dot(normed[...], w_vmem[index], preferred_element_type=jnp.float32)
         return (raw * scale).astype(jnp.bfloat16)
 
     half_planes = heads // 2
@@ -515,21 +530,28 @@
     def _():
         q_all[spare] = q_send[mirror]
 
+    def other_queries():
+        for k in range(1, half_planes):
+            q_copy(order(k)).start()
+
+        @pl.when(high)
+        def _():
+            for k in range(half_planes, heads):
+                q_copy(order(k)).start()
+
+    @pl.when(home)
+    def _():
+        other_queries()
+
+    inner = project(3).astype(jnp.float32)
+    away_only(first_sends)
+    signal_f = project(4).astype(jnp.float32)
+
     @pl.when(t != y)
     def _():
         q_copy(plane).start()
-        first_sends()
-
-    for k in range(1, half_planes):
-        q_copy(order(k)).start()
-
-    @pl.when(high)
-    def _():
-        for k in range(half_planes, heads):
-            q_copy(order(k)).start()
-
-    inner = project(3).astype(jnp.float32)
-    signal_f = project(4).astype(jnp.float32)
+        other_queries()
+
     inner_sig[...] = (inner * signal_f).astype(jnp.bfloat16)
     tail = tail_in.shape[0]
     tail_copy = remote(
@@ -553,10 +575,6 @@
         for k in range(half_planes + 1, heads):
             kv_copy(order(k)).start()
 
-    @pl.when(home)
-    def _():
-        forward_stage(spare)
-
     @pl.when(t != y)
     def _():
         kv_mirror(0).start()
@@ -569,7 +587,15 @@
     away_only(lambda: receive(plane))
     for k in range(1, half_planes):
         receive(order(k))
+    def far_slots():
+        return [order(k) for k in range(half_planes, heads)]
+
     forward_square(plane)
+
+    @pl.when(home)
+    def _():
+        forward_stage(spare)
+
     away_only(lambda: receive(spare))
 
     @pl.when(high)
@@ -578,15 +604,6 @@
 
     for k in range(1, half_planes):
         forward_square(order(k))
-    for k in range(1, half_planes):
-        receive(near(k))
-
-    @pl.when(high)
-    def _():
-        for k in range(half_planes + 1, heads):
-            receive(order(k))
-
-    forward_square(spare)
 
     span = RELAY * rows
     lane = lax.broadcasted_iota(jnp.int32, (1, lanes), 1)
@@ -759,8 +776,19 @@
             conv_out[...], wc_vmem[...], preferred_element_type=jnp.float32
         )
 
-    def far_slots():
-        return [order(k) for k in range(half_planes, heads)]
+    def turn(i):
+        return own_base + lax.rem(plane - own_base + 1 + i, half_planes)
+
+    def meet_mirror():
+        for k in range(1, half_planes):
+            receive(near(k))
+        forward_square(spare)
+
+    @pl.when(high)
+    def _():
+        meet_mirror()
+        for k in range(half_planes + 1, heads):
+            receive(order(k))
 
     for k in range(half_planes):
         finish_plane(order(k))
@@ -775,51 +803,80 @@
             attend_row(q)
             partial(q, False)
 
+    @pl.when(low)
+    def _():
+        meet_mirror()
+
     away_only(lambda: q_arrived(plane))
     for k in range(1, half_planes):
         q_arrived(order(k))
     attend_triangle(own_base)
 
+    @pl.when(high)
+    def _():
+        forward_square(mirror)
+
     @pl.when(low)
     def _():
         @pl.loop(0, half_planes)
-        def _(q):
-            finalize(q, False)
+        def _(i):
+            finalize(turn(i), False)
 
     convolve()
+
+    @pl.when(high)
+    def _():
+        finish_plane(mirror)
+        attend([(half_planes + i, mirror, False) for i in range(half_planes)])
+
     for k in range(1, half_planes):
         forward_square(near(k))
+
+    @pl.when(high)
+    def _():
+        for k in range(half_planes + 1, heads):
+            forward_square(order(k))
+
+
     for k in range(half_planes):
         finish_plane(near(k))
         if k == 0:
             away_only(lambda: q_arrived(spare))
         else:
             q_arrived(near(k))
-    attend_triangle(heads)
-
-    @pl.when(low)
-    def _():
+    @pl.loop(0, half_planes)
+    def _(i):
+        q = turn(i)
+        for row in range(half_planes):
+
+            @pl.when(q - own_base == row)
+            def _(row=row):
+                attend([(heads + row, heads + c, c == row) for c in range(row + 1)])
+
+        @pl.when(low)
+        def _():
+            finalize(q, True)
+
+        @pl.when(high)
+        def _():
+            partial(q, True)
+
+    @pl.when(high)
+    def _():
+        for slot in far_slots()[1:]:
+            finish_plane(slot)
+
+        attend(
+            [
+                (half_planes + i, slot, False)
+                for slot in far_slots()[1:]
+                for i in range(half_planes)
+            ]
+        )
+
         @pl.loop(0, half_planes)
-        def _(q):
-            finalize(q, True)
-
-    @pl.when(high)
-    def _():
-        for slot in far_slots():
-            forward_square(slot)
-
-        @pl.loop(half_planes, heads)
-        def _(q):
-            partial(q, True)
-
-        for slot in far_slots():
-            finish_plane(slot)
-
-        attend([(half_planes + i, j, False) for j in range(half_planes) for i in range(half_planes)])
-
-        @pl.loop(half_planes, heads)
-        def _(q):
-            finalize(q, False)
+        def _(i):
+            finalize(turn(i), False)
 
     weight_copies[len(sources) + 1].wait()
     half_rows = rows // 2
@@ -859,9 +916,10 @@
                 turned[:, m : m + 1] * p_all[h, held, :].astype(jnp.float32)
                 + turned[:, 2 + m : 3 + m] * p_all[second, held, :].astype(jnp.float32)
             )
-        diff = maps[0] - lam_own[:, h : h + 1] * maps[1]
+        own_lam = jnp.sum(jnp.where(lam_index == h, lam_own[...], 0.0), axis=-1, keepdims=True)
+        diff = maps[0] - own_lam * maps[1]
         mean = jnp.mean(diff * diff, axis=-1, keepdims=True)
-        part = slice(h * lanes, (h + 1) * lanes)
+        part = pl.ds(pl.multiple_of(h * lanes, lanes), lanes)
         head_out[:, part] = (diff * lax.rsqrt(mean + 1e-05) * opened[:, part]).astype(
             jnp.bfloat16
         )
@@ -876,8 +934,9 @@
 
     @pl.when(high)
     def _():
-        for h in range(half_planes):
-            merged(h)
+        @pl.loop(0, half_planes)
+        def _(i):
+            merged(lax.rem(mirror + jnp.where(home, 0, 1) + i, half_planes))
 
     conv_part[...] += jnp.dot(
         head_out[:, :split], wo_vmem[:split, :], preferred_element_type=jnp.float32
@@ -1038,7 +1097,7 @@
         + [dma((slots,)) for _ in range(18)]
         + [pltpu.SemaphoreType.REGULAR, pltpu.SemaphoreType.REGULAR],
         compiler_params=pltpu.CompilerParams(
-            collective_id=0, has_side_effects=True, vmem_limit_bytes=(60 * 1024 - 4000) * 1024
+            collective_id=0, has_side_effects=True, vmem_limit_bytes=58000 * 1024
         ),
     )(*operands)
 

time: 43.1 us -> 42.8 us (level)
  Pallas kernels: 40.9 us -> 40.3 us
    pallas_call x1, Pallas kernels: 40.9 us -> 40.3 us  [fused(): pl.pallas_call(functools.partial(fused_kernel, sp_count, heads), out_shap...]
where the time goes in v6:
time: 42.8 us; the launch traced here: 42.3 us
  Pallas kernels  40.3 us (94%)
  local copies, waits for them, and re-layouts  1.39 us (3%)
  between operations  0.64 us (1%)
    pallas_call x1, Pallas kernels, fused(): pl.pallas_call(functools.partial(fused_kernel, sp_count, heads), out_shap...  40.3 us
    unnamed x2, local copies, waits for them, and re-layouts  1.39 us

profile of v6, /device:TPU:17, one launch (start us, length us, event | category | flops | bytes accessed | tf_op | source)
XLA Modules:
  0.0 42.3 jit_solution(14030043368505083449)
XLA Ops:
  0.6 40.3 %shard_map.149 = (bf16[128,2048]{1,0:T(8,128)(2,1)S(1)}, f32[4,2,256]{2,1,0:T(2,128)S(1)}) custom-call(bf16[256,1024]{1,0:T(8,128)(2,1)} %tokens_hbm.1, f32[1,2048]{1,0:T(1,128)} %bitcast.3, bf16[2048,512]{1,0:T(8,128)(2,1)} %wq_hbm.1, bf16[2048,512]{1,0:T(8,128)(2,1)} %wk_hbm.1, bf16[2048,512]{1,0:T(8,128)(2,1)} %wv_hbm.1, bf16[2048,512]{1,0:T(8,128)(2,1)} %wg_hbm.1, ...), custom_call_target="tpu_custom_call" | custom-call | tf_op jit(solution)/shard_map/pallas_call | solution.py:1047
  40.9 0.8 %copy.18 = bf16[128,2048]{1,0:T(8,128)(2,1)} copy(bf16[128,2048]{1,0:T(8,128)(2,1)S(1)} %get-tuple-element.2) | data formatting | bytes 1048576
  41.7 0.6 %copy.19 = f32[4,2,256]{2,1,0:T(2,128)} copy(f32[4,2,256]{2,1,0:T(2,128)S(1)} %get-tuple-element.3) | data formatting | bytes 16384

commit v7 on v6

--- a/solution.py
+++ b/solution.py
@@ -777,7 +777,7 @@
         )
 
     def turn(i):
-        return own_base + lax.rem(plane - own_base + 1 + i, half_planes)
+        return own_base + lax.rem(plane - own_base + jnp.where(home, 1, 0) + i, half_planes)
 
     def meet_mirror():
         for k in range(1, half_planes):
@@ -936,7 +936,7 @@
     def _():
         @pl.loop(0, half_planes)
         def _(i):
-            merged(lax.rem(mirror + jnp.where(home, 0, 1) + i, half_planes))
+            merged(lax.rem(mirror + i, half_planes))
 
     conv_part[...] += jnp.dot(
         head_out[:, :split], wo_vmem[:split, :], preferred_element_type=jnp.float32

time: 42.8 us -> 42.6 us (level)
  no operation moved by 1% of the time
where the time goes in v7:
time: 42.6 us; the launch traced here: 42.4 us
  Pallas kernels  40.4 us (95%)
  local copies, waits for them, and re-layouts  1.39 us (3%)
  between operations  0.64 us (2%)
    pallas_call x1, Pallas kernels, fused(): pl.pallas_call(functools.partial(fused_kernel, sp_count, heads), out_shap...  40.4 us
    unnamed x2, local copies, waits for them, and re-layouts  1.39 us

profile of v7, /device:TPU:17, one launch (start us, length us, event | category | flops | bytes accessed | tf_op | source)
XLA Modules:
  0.0 42.4 jit_solution(8248261716714091874)
XLA Ops:
  0.6 40.4 %shard_map.149 = (bf16[128,2048]{1,0:T(8,128)(2,1)S(1)}, f32[4,2,256]{2,1,0:T(2,128)S(1)}) custom-call(bf16[256,1024]{1,0:T(8,128)(2,1)} %tokens_hbm.1, f32[1,2048]{1,0:T(1,128)} %bitcast.3, bf16[2048,512]{1,0:T(8,128)(2,1)} %wq_hbm.1, bf16[2048,512]{1,0:T(8,128)(2,1)} %wk_hbm.1, bf16[2048,512]{1,0:T(8,128)(2,1)} %wv_hbm.1, bf16[2048,512]{1,0:T(8,128)(2,1)} %wg_hbm.1, ...), custom_call_target="tpu_custom_call" | custom-call | tf_op jit(solution)/shard_map/pallas_call | solution.py:1047
  41.0 0.8 %copy.18 = bf16[128,2048]{1,0:T(8,128)(2,1)} copy(bf16[128,2048]{1,0:T(8,128)(2,1)S(1)} %get-tuple-element.2) | data formatting | bytes 1048576
  41.8 0.6 %copy.19 = f32[4,2,256]{2,1,0:T(2,128)} copy(f32[4,2,256]{2,1,0:T(2,128)S(1)} %get-tuple-element.3) | data formatting | bytes 16384
